TPU v7x, 32 devices: a whole 2x2x4 slice. The times are simulated.
32 devices in a mesh: grp: 2 (over y), sp: 4 (over z), tp: 4 (over x, core).
Axes of the slice: x: 2, y: 2, z: 4, core: 2. Of those that a mesh axis runs over, the one named last changes fastest.
Arguments:
- latents: bfloat16 [3072, 4096], P(('grp', 'sp', 'tp')), parts along dimension 0, may hold values from -3 to 3
- conditions: float32 [4, 4096], P('grp', 'sp'), parts along dimension 0, may hold values from -6 to 6
- context: bfloat16 [1024, 4096], P(('grp', 'sp')), parts along dimension 0, may hold values from -6 to 6
- w_shift: bfloat16 [4096, 4096], P('sp', 'tp'), may hold values from -0.09375 to 0.09375
- w_scale: bfloat16 [4096, 4096], P('sp', 'tp'), may hold values from -0.09375 to 0.09375
- w_gate: bfloat16 [4096, 4096], P('sp', 'tp'), may hold values from -0.09375 to 0.09375
- w_qdown: bfloat16 [4096, 1024], P(None, 'tp'), may hold values from -2 to 2
- w_kvdown: bfloat16 [4096, 512], P(None, 'tp'), may hold values from -2 to 2
- w_rope: bfloat16 [4096, 32], replicated, may hold values from -0.09375 to 0.09375
- q_gain: float32 [1024], replicated, may hold values from 1 to 24
- latent_norm_gain: float32 [512], replicated, may hold values from 0.1 to 1.9
- query_up_weight: bfloat16 [1024, 3072], P(None, 'tp'), may hold values from -0.1875 to 0.1875
- key_up_weight: bfloat16 [512, 2048], P(None, 'tp'), may hold values from -0.25 to 0.25
- value_up_weight: bfloat16 [512, 2048], P(None, 'tp'), may hold values from -0.25 to 0.25
- context_bias: float32 [32], P('tp'), may hold values from 0.5 to 2
- w_out: bfloat16 [2048, 4096], P(None, 'tp'), may hold values from -0.5 to 0.5
Outputs:
- mixed: bfloat16 [3072, 4096], P(('grp', 'sp', 'tp')), parts along dimension 0
There are 2 independent parts, one for each index of `grp`. A program takes and returns all parts, laid end to end along the dimension named above; an argument that names none is the same for every part. Nothing has to cross between parts.
All inputs are finite; a program needn't handle non-finite values.
Results may differ from a plain program's by a relative error of at most 0.01345.
The roundings to bfloat16 on the way count: a program that leaves them out, or rounds other values in their place, can miss the bound.
Values may be sent and summed in bfloat16 or wider, within the bound.
A program may use at most 64 MiB of HBM per device.

v0:
```python
import functools

import jax
import jax.numpy as jnp
import numpy as np
from jax import lax
from jax.experimental import pallas as pl
from jax.experimental.pallas import tpu as pltpu
from jax.sharding import PartitionSpec as P

PLAIN_QK_DIM = 64
ROTARY_DIM = 32
VALUE_DIM = 64
GRID_W = 64


EPSILON = 1e-06
NEGATIVE = -1e30


def layer_modulate(row_block, shift_by, scale_by):
    values = row_block.astype(jnp.float32)
    center = values - jnp.mean(values, axis=-1, keepdims=True)
    spread = jnp.mean(center * center, axis=-1, keepdims=True)
    normed = center * lax.rsqrt(spread + EPSILON)
    return (normed * (1.0 + scale_by) + shift_by).astype(jnp.bfloat16)


def rms_scale(raw_rows, gain_vec):
    values = raw_rows.astype(jnp.float32)
    factor = lax.rsqrt(jnp.mean(values * values, axis=-1, keepdims=True) + EPSILON)
    return (values * factor * gain_vec).astype(jnp.bfloat16)


def axial_turn(values, positions):
    freq_count = values.shape[-1] // 4
    inverse = 10000.0 ** (-jnp.arange(freq_count, dtype=jnp.float32) / freq_count)
    grid_row = (positions // GRID_W).astype(jnp.float32)
    grid_col = (positions % GRID_W).astype(jnp.float32)
    target = (positions.shape[0],) + (1,) * (values.ndim - 2) + (freq_count,)
    pieces = []
    for half_index, coordinate in enumerate((grid_row, grid_col)):
        angles = (coordinate[:, None] * inverse[None, :]).reshape(target)
        cosine = jnp.cos(angles)
        sine_of = jnp.sin(angles)
        segment = values[..., 2 * half_index * freq_count : 2 * (half_index + 1) * freq_count]
        low_half = segment[..., :freq_count]
        high_half = segment[..., freq_count:]
        pieces.append(low_half * cosine - high_half * sine_of)
        pieces.append(low_half * sine_of + high_half * cosine)
    return jnp.concatenate(pieces, axis=-1)


def plain_device(
    latents,
    conditions,
    context,
    w_shift,
    w_scale,
    w_gate,
    w_qdown,
    w_kvdown,
    w_rope,
    q_gain,
    latent_norm_gain,
    query_up_weight,
    key_up_weight,
    value_up_weight,
    context_bias,
    w_out,
):
    tp_count = lax.axis_size("tp")
    tp_index = lax.axis_index("tp")
    sp_index = lax.axis_index("sp")
    own_rows = latents.shape[0]
    tok_count = own_rows * tp_count
    ctx_share = context.shape[0] // tp_count
    cond_act = jax.nn.silu(conditions).astype(jnp.bfloat16)
    partial_mod = jnp.concatenate(
        [
            jnp.dot(cond_act, w_shift, preferred_element_type=jnp.float32),
            jnp.dot(cond_act, w_scale, preferred_element_type=jnp.float32),
            jnp.dot(cond_act[0:1], w_gate, preferred_element_type=jnp.float32),
        ],
        axis=0,
    )
    summed = lax.psum(partial_mod, "sp")
    modulation = lax.all_gather(summed, "tp", axis=1, tiled=True)
    ctx_own = lax.dynamic_slice_in_dim(context, tp_index * ctx_share, ctx_share, 0)
    h_lat = layer_modulate(latents, modulation[0], modulation[2])
    h_ctx = layer_modulate(ctx_own, modulation[1], modulation[3])
    h_own = jnp.concatenate([h_lat, h_ctx], axis=0)
    rope_raw = jnp.dot(h_own, w_rope, preferred_element_type=jnp.float32)
    own_pos = sp_index * tok_count + tp_index * own_rows + jnp.arange(own_rows, dtype=jnp.int32)
    kr_lat = axial_turn(rope_raw[:own_rows], own_pos).astype(jnp.bfloat16)
    kr_ctx = rope_raw[own_rows:].astype(jnp.bfloat16)
    arrived = lax.all_gather(h_own, "tp", axis=0, tiled=True)
    projected = jnp.concatenate(
        [
            jnp.dot(arrived, w_qdown, preferred_element_type=jnp.float32),
            jnp.dot(arrived, w_kvdown, preferred_element_type=jnp.float32),
        ],
        axis=1,
    ).astype(jnp.bfloat16)
    q_cols = w_qdown.shape[1]
    grouped = projected.reshape(tp_count, own_rows + ctx_share, projected.shape[1])
    cq_cols = grouped[:, :own_rows, :q_cols].reshape(tok_count, q_cols)
    kvl_cols = grouped[:, :own_rows, q_cols:].reshape(tok_count, w_kvdown.shape[1])
    kvc_cols = grouped[:, own_rows:, q_cols:].reshape(tp_count * ctx_share, w_kvdown.shape[1])
    cq_raw, kvl_raw, kvc_raw, krl_all, krc_all = (
        lax.all_gather(cq_cols, "tp", axis=1, tiled=True),
        lax.all_gather(kvl_cols, "tp", axis=1, tiled=True),
        lax.all_gather(kvc_cols, "tp", axis=1, tiled=True),
        lax.all_gather(kr_lat, "tp", axis=0, tiled=True),
        lax.all_gather(kr_ctx, "tp", axis=0, tiled=True),
    )
    cq_all = rms_scale(cq_raw, q_gain)
    ckv_all = jnp.concatenate(
        [rms_scale(kvl_raw, latent_norm_gain), rms_scale(kvc_raw, latent_norm_gain)], axis=0
    )
    kr_all = jnp.concatenate([krl_all, krc_all], axis=0)
    head_count = query_up_weight.shape[1] // (PLAIN_QK_DIM + ROTARY_DIM)
    q_all = jnp.dot(cq_all, query_up_weight, preferred_element_type=jnp.float32)
    q_all = q_all.reshape(tok_count, head_count, PLAIN_QK_DIM + ROTARY_DIM)
    query_pos = sp_index * tok_count + jnp.arange(tok_count, dtype=jnp.int32)
    queries = jnp.concatenate(
        [q_all[..., :PLAIN_QK_DIM], axial_turn(q_all[..., PLAIN_QK_DIM:], query_pos)], axis=-1
    ).astype(jnp.bfloat16)
    q_nope = queries[..., :PLAIN_QK_DIM]
    q_rope = queries[..., PLAIN_QK_DIM:]
    seg_rows = ckv_all.shape[0]
    is_ctx = (jnp.arange(seg_rows, dtype=jnp.int32) >= tok_count).astype(jnp.float32)
    bias_row = context_bias[None, :, None] * is_ctx[None, None, :]
    score_scale = (PLAIN_QK_DIM + ROTARY_DIM) ** (-0.5)

    def attend_block(running, key_block, value_block, rope_block):
        running_max, running_sum, numerator = running
        scores = jnp.einsum("ihd,jhd->ihj", q_nope, key_block, preferred_element_type=jnp.float32)
        scores = scores + jnp.einsum(
            "ihd,jd->ihj", q_rope, rope_block, preferred_element_type=jnp.float32
        )
        scores = scores * score_scale + bias_row
        new_max = jnp.maximum(running_max, jnp.max(scores, axis=-1))
        rescale = jnp.exp(running_max - new_max)
        exponent = jnp.exp(scores - new_max[..., None])
        running_sum = running_sum * rescale + jnp.sum(exponent, axis=-1)
        numerator = numerator * rescale[..., None] + jnp.einsum(
            "ihj,jhd->ihd",
            exponent.astype(jnp.bfloat16),
            value_block,
            preferred_element_type=jnp.float32,
        )
        return (new_max, running_sum, numerator)

    initial = (
        jnp.full((tok_count, head_count), NEGATIVE, jnp.float32),
        jnp.zeros((tok_count, head_count), jnp.float32),
        jnp.zeros((tok_count, head_count, VALUE_DIM), jnp.float32),
    )

    def expand_latent(key_group):
        latent_rows, rope_block = key_group
        key_block = jnp.dot(latent_rows, key_up_weight, preferred_element_type=jnp.float32).astype(
            jnp.bfloat16
        )
        value_block = jnp.dot(
            latent_rows, value_up_weight, preferred_element_type=jnp.float32
        ).astype(jnp.bfloat16)
        return (
            key_block.reshape(seg_rows, head_count, PLAIN_QK_DIM),
            value_block.reshape(seg_rows, head_count, VALUE_DIM),
            rope_block,
        )

    members = (
        lax.all_gather(ckv_all, "sp", axis=0, tiled=True),
        lax.all_gather(kr_all, "sp", axis=0, tiled=True),
    )
    block_count = members[0].shape[0] // seg_rows
    stacked = tuple(
        (member.reshape((block_count, seg_rows) + member.shape[1:]) for member in members)
    )

    def step_fn(state, key_group):
        key_block, value_block, rope_block = expand_latent(key_group)
        return (attend_block(state, key_block, value_block, rope_block), None)

    result, unused = lax.scan(step_fn, initial, stacked)
    running_max, running_sum, numerator = result
    attended = (
        (numerator / running_sum[..., None])
        .astype(jnp.bfloat16)
        .reshape(tok_count, head_count * VALUE_DIM)
    )
    proj_cols = jnp.dot(
        lax.all_gather(attended, "tp", axis=1, tiled=True),
        w_out,
        preferred_element_type=jnp.float32,
    )
    proj_rows = lax.all_to_all(
        proj_cols.astype(jnp.bfloat16), "tp", split_axis=0, concat_axis=1, tiled=True
    )
    mixed_rows = latents.astype(jnp.float32) + modulation[4] * proj_rows.astype(jnp.float32)
    return mixed_rows.astype(jnp.bfloat16)


MESH = pl.DeviceIdType.MESH
LOG2E = 1.4426950408889634
STEP = 16
BAND = 32


def turn_tables(tokens):
    freq_count = ROTARY_DIM // 4
    inverse = 10000.0 ** (-np.arange(freq_count) / freq_count)
    position = np.arange(tokens)
    cosine = np.zeros((tokens, 128), np.float32)
    sine = np.zeros((tokens, 128), np.float32)
    cosine[:, :PLAIN_QK_DIM] = 1.0
    for half_index, coordinate in enumerate((position // GRID_W, position % GRID_W)):
        angles = coordinate[:, None] * inverse[None, :]
        low = PLAIN_QK_DIM + 2 * half_index * freq_count
        high = low + freq_count
        cosine[:, low : low + freq_count] = np.cos(angles)
        cosine[:, high : high + freq_count] = np.cos(angles)
        sine[:, low : low + freq_count] = -np.sin(angles)
        sine[:, high : high + freq_count] = np.sin(angles)
    return cosine, sine


def lanes_of(shape):
    return lax.broadcasted_iota(jnp.int32, shape, len(shape) - 1)


def turned(values, cosine, sine):
    lane = lanes_of(values.shape)
    swapped = jnp.where(
        (lane // 8) % 2 == 0, pltpu.roll(values, 120, 1), pltpu.roll(values, 8, 1)
    )
    return values * cosine + swapped * sine


def block_kernel(
    cond_ref,
    bias_ref,
    qgain_ref,
    kvgain_ref,
    rope_ref,
    lat_hbm,
    ctx_hbm,
    wsh_hbm,
    wsc_hbm,
    wga_hbm,
    wqd_hbm,
    wkd_hbm,
    wqu_hbm,
    wku_hbm,
    wvu_hbm,
    wo_hbm,
    cos_hbm,
    sin_hbm,
    out_ref,
    cond16,
    w3,
    lat,
    ctx,
    hid,
    wqd,
    wkvr,
    modp,
    mod,
    cq,
    kv,
    kvc,
    kraw,
    ck,
    cqn,
    wqu,
    wku,
    wvu,
    wo,
    cosv,
    sinv,
    qh,
    kb,
    vb,
    acc,
    mx,
    att,
    po,
    pr,
    st_mean,
    st_rate,
    part,
    load_sem,
    send_sem,
    recv_sem,
    zsend,
    zrecv,
    dsend,
    drecv,
):
    f32, bf16 = jnp.float32, jnp.bfloat16
    spn = lax.axis_size("sp")
    p = lax.axis_index("tp")
    z = lax.axis_index("sp")
    core = lax.rem(p, 2)
    side = p // 2
    p1, p2, p3 = p ^ 1, p ^ 2, p ^ 3
    own = lat.shape[1]
    width = lat.shape[2]
    tok = own * 4
    pair = own * 2
    ctxn = ctx.shape[0]
    seg = tok + ctxn
    modw = w3.shape[2]
    heads = qh.shape[0]
    hrow = seg // 2
    qcols = cq.shape[3]
    kcols = kv.shape[3]
    krank = 4 * kcols

    loads = []

    def load(src, dst):
        copy = pltpu.make_async_copy(src, dst, load_sem.at[len(loads)])
        loads.append(copy)
        copy.start()
        return copy

    l_lat = load(lat_hbm, lat.at[p])
    l_w3 = [load(ref, w3.at[i]) for i, ref in enumerate((wsh_hbm, wsc_hbm, wga_hbm))]
    l_ctx = load(ctx_hbm, ctx)
    l_kd = load(wkd_hbm, wkvr.at[:, pl.ds(0, kcols)])
    l_qd = load(wqd_hbm, wqd)
    table_rows = pl.ds(pl.multiple_of(z * tok, 8), tok)
    l_cos = load(cos_hbm.at[table_rows], cosv)
    l_sin = load(sin_hbm.at[table_rows], sinv)
    l_ku = load(wku_hbm, wku)
    l_vu = load(wvu_hbm, wvu)
    l_qu = load(wqu_hbm, wqu)
    l_wo = load(wo_hbm, wo)

    barrier = pltpu.get_barrier_semaphore()
    for peer in (p1, p2, p3):
        pl.semaphore_signal(barrier, inc=1, device_id={"tp": peer}, device_id_type=MESH)
    for d in range(1, spn):
        pl.semaphore_signal(
            barrier, inc=1, device_id={"sp": lax.rem(z + d, spn)}, device_id_type=MESH
        )

    sends = []

    def remote(src, dst, index, target):
        return pltpu.make_async_remote_copy(
            src_ref=src,
            dst_ref=dst,
            send_sem=send_sem.at[index],
            recv_sem=recv_sem.at[index],
            device_id=target,
            device_id_type=MESH,
        )

    def send(src, dst, index, target):
        copy = remote(src, dst, index, target)
        copy.start()
        sends.append(copy)
        return copy

    counter = [0]

    def fresh():
        counter[0] += 1
        return counter[0] - 1

    def spread(view, far_view=None):
        far_view = far_view or view
        i1, i2, i3 = fresh(), fresh(), fresh()
        first = send(view(p), view(p), i2, {"tp": p2})
        second = send(view(p), view(p), i1, {"tp": p1})

        def relay():
            first.wait_recv()
            third = send(far_view(p2), far_view(p2), i3, {"tp": p1})
            return third.wait_recv

        return relay, second.wait_recv

    cond16[...] = jnp.zeros_like(cond16)
    cond16[0:2, :] = cond_ref[...]
    conditions = cond16[...]
    act = (conditions / (1.0 + jnp.exp(-conditions))).astype(bf16)

    pl.semaphore_wait(barrier, 3 + spn - 1)
    def near(view):
        return send(view(p), view(p), fresh(), {"tp": p1}).wait_recv

    def far(view):
        i2, i3 = fresh(), fresh()
        first = send(view(p), view(p), i2, {"tp": p2})

        def relay():
            first.wait_recv()
            return send(view(p2), view(p2), i3, {"tp": p1}).wait_recv

        return relay

    l_lat.wait()
    lat_near = near(lambda slot: lat.at[slot])
    lat_rows = [slice(r, r + BAND) for r in range(0, own, BAND)]
    lat_views = [lambda slot, r=r: lat.at[slot, pl.ds(r.start, BAND)] for r in lat_rows]
    lat_relay = [far(lat_views[0])]

    for i in range(3):
        l_w3[i].wait()
        partial_mod = jnp.dot(act, w3[i], preferred_element_type=f32)
        modp[z, 2 * i : 2 * i + 2, :] = partial_mod[0:2]
    modp[z, 6:8, :] = jnp.zeros((2, modw), f32)
    mod_waits = []
    for d in range(1, spn):
        mod_waits.append(
            send(modp.at[z], modp.at[z], fresh(), {"sp": lax.rem(z + d, spn)})
        )
    wkvr[:, kcols + ROTARY_DIM :] = jnp.zeros((width, wkvr.shape[1] - kcols - ROTARY_DIM), bf16)
    wkvr[:, kcols : kcols + ROTARY_DIM] = rope_ref[...]

    def measured(src, row_count, dst_row):
        @pl.loop(0, row_count // BAND)
        def _(i):
            rows = pl.ds(pl.multiple_of(i * BAND, BAND), BAND)
            to = pl.ds(pl.multiple_of(dst_row + i * BAND, BAND), BAND)
            tiles = [slice(c, c + 128) for c in range(0, width, 128)]
            sums = jnp.zeros((BAND, 128), f32)
            for c in tiles:
                sums = sums + src[rows, c].astype(f32)
            mean = jnp.broadcast_to(
                jnp.sum(sums, axis=-1, keepdims=True) * (1.0 / width), (BAND, 128)
            )
            squares = jnp.zeros((BAND, 128), f32)
            for c in tiles:
                center = src[rows, c].astype(f32) - mean
                squares = squares + center * center
            spread_of = jnp.sum(squares, axis=-1, keepdims=True) * (1.0 / width)
            st_mean[to, :] = mean
            st_rate[to, :] = jnp.broadcast_to(lax.rsqrt(spread_of + EPSILON), (BAND, 128))

    def modulate(src, row_count, dst_row, which):
        @pl.loop(0, row_count // BAND)
        def _(i):
            rows = pl.ds(pl.multiple_of(i * BAND, BAND), BAND)
            to = pl.ds(pl.multiple_of(dst_row + i * BAND, BAND), BAND)
            mean, rate = st_mean[to, :], st_rate[to, :]
            for c in range(0, width, 128):
                j, k = c // modw, c % modw
                shift_by = mod[j, which : which + 1, k : k + 128]
                scale_by = mod[j, 2 + which : 3 + which, k : k + 128]
                normed = (src[rows, c : c + 128].astype(f32) - mean) * rate
                hid[to, c : c + 128] = (normed * (1.0 + scale_by) + shift_by).astype(bf16)

    measured(lat.at[p], own, p * own)
    l_ctx.wait()
    measured(ctx, ctxn, tok)
    for copy in mod_waits:
        copy.wait_recv()
    total = modp[0]
    for i in range(1, spn):
        total = total + modp[i]
    mod[p] = total
    mod_waits = [send(mod.at[p], mod.at[p], fresh(), {"tp": peer}) for peer in (p2, p3, p1)]
    for view in lat_views[1:]:
        lat_relay.append(far(view))
    lat_near()
    measured(lat.at[p1], own, p1 * own)
    lat_far = [lat_relay[0]()]
    for copy in mod_waits:
        copy.wait_recv()

    modulate(ctx, ctxn, tok, 1)
    l_kd.wait()
    l_qd.wait()
    mixed_ctx = jnp.dot(hid[tok:, :], wkvr[...], preferred_element_type=f32)
    kvc[p] = mixed_ctx[:, :kcols].astype(bf16)
    kraw[tok:, :] = mixed_ctx[:, kcols:]
    relays = [spread(lambda slot: kvc.at[slot])]

    modulate(lat.at[p], own, p * own, 0)
    modulate(lat.at[p1], own, p1 * own, 0)

    def down(half):
        rows = pl.ds(pl.multiple_of(half * pair, STEP), pair)
        both = jnp.dot(hid[rows, :], wkvr[...], preferred_element_type=f32)
        kv[p, half] = both[:, :kcols].astype(bf16)
        kraw[rows, :] = both[:, kcols:]
        one = spread(lambda slot: kv.at[slot, half], lambda slot: kv.at[slot, 1 - half])
        cq[p, half] = jnp.dot(hid[rows, :], wqd[...], preferred_element_type=f32).astype(bf16)
        return one, spread(lambda slot: cq.at[slot, half], lambda slot: cq.at[slot, 1 - half])

    kv_a, cq_a = down(side)
    for n, r in enumerate(lat_rows):
        if n:
            lat_far.append(lat_relay[n]())
        piece = lat.at[p2, pl.ds(r.start, BAND)]
        measured(piece, BAND, p2 * own + r.start)
        modulate(piece, BAND, p2 * own + r.start, 0)
    for n, r in enumerate(lat_rows):
        lat_far[n]()
        piece = lat.at[p3, pl.ds(r.start, BAND)]
        measured(piece, BAND, p3 * own + r.start)
        modulate(piece, BAND, p3 * own + r.start, 0)
    kv_b, cq_b = down(1 - side)
    relays += [kv_a, kv_b]
    kv_far = [r() for r, _ in relays]
    for w in kv_far:
        w()
    for _, w in relays:
        w()

    l_cos.wait()
    l_sin.wait()
    kr_lat = turned(pltpu.roll(kraw[:tok, :], 64, 1), cosv[...], sinv[...])
    kraw[:tok, :] = kr_lat
    kraw[tok:, :] = pltpu.roll(kraw[tok:, :], 64, 1)
    for hf in range(2):
        for t in range(4):
            packed = None
            for j in range(4):
                first_row = hf * hrow + (4 * t + j) * STEP
                moved = pltpu.roll(
                    kraw[first_row : first_row + STEP, :], (32 * j + 64) % 128, 1
                )
                packed = moved if packed is None else packed + moved
            ck[z, hf, hrow : hrow + STEP, 128 * t : 128 * t + 128] = packed.astype(bf16)

    def rms(pieces, gain_ref, store):
        values = [piece.astype(f32) for piece in pieces]
        total_of = None
        for v in values:
            s = jnp.sum(v * v, axis=-1, keepdims=True)
            total_of = s if total_of is None else total_of + s
        cols = values[0].shape[1]
        factor = lax.rsqrt(total_of / (cols * len(values)) + EPSILON)
        for j, v in enumerate(values):
            gain = gain_ref[0:1, j * cols : (j + 1) * cols]
            store(slice(j * cols, (j + 1) * cols), (v * factor * gain).astype(bf16))

    for piece in range(seg // 64):
        base = piece * 64
        if base < tok:
            chunk = [kv[r, base // pair, base % pair : base % pair + 64, :] for r in range(4)]
        else:
            chunk = [kvc[r, base - tok : base - tok + 64, :] for r in range(4)]

        def put(cols, value, base=base):
            ck[z, base // hrow, base % hrow : base % hrow + 64, cols] = value

        rms(chunk, kvgain_ref, put)

    def hop(origin, target, way):
        return pltpu.make_async_remote_copy(
            src_ref=ck.at[origin, core],
            dst_ref=ck.at[origin, core],
            send_sem=zsend.at[way, origin],
            recv_sem=zrecv.at[origin],
            device_id={"sp": target},
            device_id_type=MESH,
        )

    def cross(origin, half):
        return pltpu.make_async_remote_copy(
            src_ref=ck.at[origin, half],
            dst_ref=ck.at[origin, half],
            send_sem=dsend.at[origin],
            recv_sem=drecv.at[origin],
            device_id={"tp": p1},
            device_id_type=MESH,
        )

    has_right = z + 1 < spn
    has_left = z >= 1

    @pl.when(has_right)
    def _():
        hop(z, z + 1, 0).start()

    @pl.when(has_left)
    def _():
        hop(z, z - 1, 1).start()

    w_cq = [cq_a[0](), cq_b[0]()]
    for w in w_cq:
        w()
    cq_a[1]()
    cq_b[1]()
    for piece in range(tok // 64):
        base = piece * 64
        chunk = [cq[r, base // pair, base % pair : base % pair + 64, :] for r in range(4)]

        def put(cols, value, base=base):
            cqn[base : base + 64, cols] = value

        rms(chunk, qgain_ref, put)
    l_qu.wait()
    q_all = jnp.dot(cqn[...], wqu[...], preferred_element_type=f32)
    lane = lanes_of((tok, 128))
    for h in range(heads):
        offset = h * (PLAIN_QK_DIM + ROTARY_DIM)
        tile, shift = offset // 128, offset % 128
        head = q_all[:, 128 * tile : 128 * tile + 128]
        if shift:
            head = pltpu.roll(head, 128 - shift, 1)
            if shift + PLAIN_QK_DIM + ROTARY_DIM > 128:
                rest = pltpu.roll(q_all[:, 128 * tile + 128 : 128 * tile + 256], 128 - shift, 1)
                head = jnp.where(lane < 128 - shift, head, rest)
        qh[h] = turned(head, cosv[...], sinv[...]).astype(bf16)
    l_ku.wait()
    l_vu.wait()
    acc[...] = jnp.zeros_like(acc)
    mx[...] = jnp.full(mx.shape, NEGATIVE, f32)
    factor = (PLAIN_QK_DIM + ROTARY_DIM) ** (-0.5) * LOG2E

    def arrive(step):
        left, right = z - 1 - step, z + 1 + step

        @pl.when(left >= 0)
        def _():
            hop(left, z, 0).wait_recv()
            cross(left, core).start()

            @pl.when(has_right)
            def _():
                hop(left, z + 1, 0).start()

        @pl.when(right < spn)
        def _():
            hop(right, z, 1).wait_recv()
            cross(right, core).start()

            @pl.when(has_left)
            def _():
                hop(right, z - 1, 1).start()

    def expand(block):
        lane_h = lanes_of((hrow, 128))
        ones = (lane_h == VALUE_DIM).astype(f32)
        lane_s = lanes_of((STEP, 128))
        on_rope = (lane_s >= PLAIN_QK_DIM) & (lane_s < PLAIN_QK_DIM + ROTARY_DIM)
        for hf in range(2):
            rows = slice(hf * hrow, (hf + 1) * hrow)
            latent_rows = ck[block, hf, :hrow, :]
            pieces = []
            for t in range(4):
                packed = ck[block, hf, hrow : hrow + STEP, 128 * t : 128 * t + 128].astype(f32)
                for j in range(4):
                    moved = pltpu.roll(packed, (192 - 32 * j) % 128, 1)
                    pieces.append(jnp.where(on_rope, moved, 0.0))
            rope_key = jnp.concatenate(pieces, axis=0)
            keys = jnp.dot(latent_rows, wku[...], preferred_element_type=f32)
            vals = jnp.dot(latent_rows, wvu[...], preferred_element_type=f32)
            for hp in range(heads // 2):
                cols = slice(128 * hp, 128 * hp + 128)
                k2, v2 = keys[:, cols], vals[:, cols]
                kb[2 * hp, rows, :] = jnp.where(lane_h < 64, k2, rope_key).astype(bf16)
                kb[2 * hp + 1, rows, :] = jnp.where(
                    lane_h < 64, pltpu.roll(k2, 64, 1), rope_key
                ).astype(bf16)
                vb[2 * hp, rows, :] = jnp.where(lane_h < 64, v2, ones).astype(bf16)
                vb[2 * hp + 1, rows, :] = jnp.where(
                    lane_h < 64, pltpu.roll(v2, 64, 1), ones
                ).astype(bf16)

    def score(h):
        return lax.dot_general(
            qh[h], kb[h], (((1,), (1,)), ((), ())), preferred_element_type=f32
        )

    def attend(h, scores):
        tiles = [scores[:, c : c + 128] * factor for c in range(0, seg, 128)]
        bias = bias_ref[h] * LOG2E
        tiles = [t + bias if n * 128 >= tok else t for n, t in enumerate(tiles)]
        best = functools.reduce(jnp.maximum, tiles)
        old = mx[h]
        new = jnp.maximum(old, jnp.max(best, axis=-1, keepdims=True))
        mx[h] = new
        weights = jnp.concatenate([jnp.exp2(t - new).astype(bf16) for t in tiles], axis=1)
        acc[h] = acc[h] * jnp.exp2(old - new) + jnp.dot(
            weights, vb[h], preferred_element_type=f32
        )

    def attend_all(after):
        scores = score(0)
        for h in range(heads):
            following = score(h + 1) if h + 1 < heads else None
            attend(h, scores)
            after(h)
            scores = following

    def block_at(step):
        below = jnp.minimum(z, spn - 1 - z)
        near = jnp.where(lax.rem(step, 2) == 1, z - (step + 1) // 2, z + step // 2)
        past = jnp.where(z < spn - 1 - z, step, spn - 1 - step)
        return jnp.where(step <= 2 * below, near, past)

    @pl.loop(0, spn - 1)
    def _(step):
        @pl.when(step > 0)
        def _():
            arrive(step - 1)

        block = block_at(step)

        @pl.when(step > 0)
        def _():
            cross(block, 1 - core).wait_recv()

        expand(block)
        attend_all(lambda h: None)

    att_relay, att_near = [], []
    lane64 = lane < 64

    def finish(h):
        if h % 2 == 0:
            return
        hp = h // 2
        outs = []
        for g in (h - 1, h):
            a = acc[g]
            outs.append(a / a[:, VALUE_DIM : VALUE_DIM + 1])
        att[p, hp] = jnp.where(lane64, outs[0], pltpu.roll(outs[1], 64, 1)).astype(bf16)
        att_relay.append(far(lambda slot: att.at[slot, hp]))
        att_near.append(near(lambda slot: att.at[slot, hp]))

    arrive(spn - 2)
    last_block = block_at(jnp.int32(spn - 1))
    cross(last_block, 1 - core).wait_recv()
    expand(last_block)
    attend_all(finish)

    l_wo.wait()
    half_k = heads * VALUE_DIM * 2
    order = (p2, p3, p1, p)

    def project(dest, chip):
        rows = pl.ds(pl.multiple_of(dest * own, STEP), own)
        joined = jnp.concatenate(
            [att[2 * chip + r, hp, rows, :] for r in range(2) for hp in range(heads // 2)], axis=1
        )
        k_rows = pl.ds(pl.multiple_of(chip * half_k, 128), half_k)
        return jnp.dot(joined, wo[k_rows, :], preferred_element_type=f32)

    att_far = [att_relay[0](), att_relay[1]()]
    for w in att_near:
        w()
    for dest in order:
        part[dest] = project(dest, side)
    att_far += [r() for r in att_relay[2:]]
    for w in att_far:
        w()
    final = []
    for dest in order:
        made = (part[dest] + project(dest, 1 - side)).astype(bf16)
        if dest is p:
            pr[p] = made
        else:
            po[dest] = made
            final.append(send(po.at[dest], pr.at[p], fresh(), {"tp": dest}))
    for copy in final:
        copy.wait_recv()

    @pl.loop(0, own // STEP)
    def _(i):
        rows = pl.ds(pl.multiple_of(i * STEP, STEP), STEP)
        for j in range(4):
            cols = slice(j * modw, (j + 1) * modw)
            gate = mod[j, 4:5, :]
            out_ref[rows, cols] = (
                lat[p, rows, cols].astype(f32) + gate * pr[j, rows, :].astype(f32)
            ).astype(bf16)

    for copy in sends:
        copy.wait_send()

    @pl.when(has_right)
    def _():
        hop(z, z + 1, 0).wait_send()

    @pl.when(has_left)
    def _():
        hop(z, z - 1, 1).wait_send()

    for step in range(spn - 1):
        left, right = z - 1 - step, z + 1 + step

        @pl.when(left >= 0)
        def _():
            cross(left, core).wait_send()

            @pl.when(has_right)
            def _():
                hop(left, z + 1, 0).wait_send()

        @pl.when(right < spn)
        def _():
            cross(right, core).wait_send()

            @pl.when(has_left)
            def _():
                hop(right, z - 1, 1).wait_send()


def fused_device(
    latents,
    conditions,
    context,
    w_shift,
    w_scale,
    w_gate,
    w_qdown,
    w_kvdown,
    w_rope,
    q_gain,
    latent_norm_gain,
    query_up_weight,
    key_up_weight,
    value_up_weight,
    context_bias,
    w_out,
):
    f32, bf16 = jnp.float32, jnp.bfloat16
    spn = lax.axis_size("sp")
    own, width = latents.shape
    ctxn = context.shape[0]
    tok = 4 * own
    seg = tok + ctxn
    heads = context_bias.shape[0]
    modw = w_shift.shape[1]
    kdim, qcols = w_qdown.shape
    kcols = w_kvdown.shape[1]
    cosine, sine = turn_tables(tok * spn)
    vmem = pl.BlockSpec(memory_space=pltpu.VMEM)
    smem = pl.BlockSpec(memory_space=pltpu.SMEM)
    hbm = pl.BlockSpec(memory_space=pl.ANY)
    V, DMA = pltpu.VMEM, pltpu.SemaphoreType.DMA
    scratch = [
        V((16, conditions.shape[1]), f32),
        V((3,) + w_shift.shape, bf16),
        V((4, own, width), bf16),
        V((ctxn, width), bf16),
        V((seg, width), bf16),
        V((kdim, qcols), bf16),
        V((kdim, kcols + 128), bf16),
        V((spn, 8, modw), f32),
        V((4, 8, modw), f32),
        V((4, 2, 2 * own, qcols), bf16),
        V((4, 2, 2 * own, kcols), bf16),
        V((4, ctxn, kcols), bf16),
        V((seg, 128), f32),
        V((spn, 2, seg // 2 + STEP, 4 * kcols), bf16),
        V((tok, 4 * qcols), bf16),
        V(query_up_weight.shape, bf16),
        V(key_up_weight.shape, bf16),
        V(value_up_weight.shape, bf16),
        V(w_out.shape, bf16),
        V((tok, 128), f32),
        V((tok, 128), f32),
        V((heads, tok, 128), bf16),
        V((heads, seg, 128), bf16),
        V((heads, seg, 128), bf16),
        V((heads, tok, 128), f32),
        V((heads, tok, 128), f32),
        V((4, heads // 2, tok, 128), bf16),
        V((4, own, modw), bf16),
        V((4, own, modw), bf16),
        V((seg, 128), f32),
        V((seg, 128), f32),
        V((4, own, modw), f32),
        DMA((13,)),
        DMA((48,)),
        DMA((48,)),
        DMA((2, spn)),
        DMA((spn,)),
        DMA((spn,)),
        DMA((spn,)),
    ]
    return pl.pallas_call(
        block_kernel,
        out_shape=jax.ShapeDtypeStruct(latents.shape, bf16),
        in_specs=[vmem, smem, vmem, vmem, vmem] + [hbm] * 13,
        out_specs=vmem,
        scratch_shapes=scratch,
        compiler_params=pltpu.CompilerParams(
            collective_id=0, has_side_effects=True, vmem_limit_bytes=60 * 1024 * 1024
        ),
    )(
        conditions,
        context_bias,
        q_gain[None, :],
        latent_norm_gain[None, :],
        w_rope,
        latents,
        context,
        w_shift,
        w_scale,
        w_gate,
        w_qdown,
        w_kvdown,
        query_up_weight,
        key_up_weight,
        value_up_weight,
        w_out,
        jnp.asarray(cosine),
        jnp.asarray(sine),
    )


def on_device(*arrays):
    latents, context, bias = arrays[0], arrays[2], arrays[14]
    fits = (
        lax.axis_size("tp") == 4
        and latents.shape[0] % 32 == 0
        and context.shape[0] % 64 == 0
        and (4 * latents.shape[0] + context.shape[0]) == 512
        and arrays[6].shape[1] == 256
        and arrays[7].shape[1] == 128
        and bias.shape[0] == 8
    )
    return fused_device(*arrays) if fits else plain_device(*arrays)


def solution(mesh):
    in_specs = (
        P(("grp", "sp", "tp"), None),
        P("grp", "sp"),
        P(("grp", "sp"), None),
        P("sp", "tp"),
        P("sp", "tp"),
        P("sp", "tp"),
        P(None, "tp"),
        P(None, "tp"),
        P(),
        P(),
        P(),
        P(None, "tp"),
        P(None, "tp"),
        P(None, "tp"),
        P("tp"),
        P(None, "tp"),
    )
    out_specs = P(("grp", "sp", "tp"), None)
    return jax.shard_map(
        on_device, mesh=mesh, in_specs=in_specs, out_specs=out_specs, check_vma=False
    )
```

profile of v0, /device:TPU:0, one launch (start us, length us, event | category | flops | bytes accessed | tf_op | source)
XLA Modules:
  0.0 87.8 jit_solution(1170116792326245436)
XLA Ops:
  0.0 2.3 %copy.19.rope_ref = bf16[4096,32]{1,0:T(8,128)(2,1)} copy(bf16[4096,32]{0,1:T(8,128)(2,1)} %param.26) | data formatting | bytes 524288 | tf_op args[8]
  2.3 83.5 %shard_map.172 = bf16[96,4096]{1,0:T(8,128)(2,1)} custom-call(f32[2,1024]{1,0:T(2,128)} %cond_ref.1, f32[8]{0:T(128)} %bias_ref.1, f32[1,1024]{1,0:T(1,128)} %bitcast.2, f32[1,512]{1,0:T(1,128)} %bitcast.3, bf16[4096,32]{1,0:T(8,128)(2,1)} %copy.19.rope_ref, bf16[96,4096]{1,0:T(8,128)(2,1)} %lat_hbm.1, bf16[128,4096]{1,0:T(8,128)(2,1)} %ctx_hbm.1, ...), custom_call_target="tpu_custom_call" | custom-call | tf_op jit(solution)/shard_map/pallas_call | solution.py:885
  85.8 2.1 %copy.21 = bf16[96,4096]{1,0:T(8,128)(2,1)} copy(bf16[96,4096]{1,0:T(8,128)(2,1)} %shard_map.172) | data formatting | bytes 1572864
where the time goes:
time: 88.2 us; the launch traced here: 87.8 us
  Pallas kernels  83.5 us (95%)
  local copies, waits for them, and re-layouts  4.35 us (5%)
    pallas_call x1, Pallas kernels, fused_device(): pl.pallas_call(block_kernel, out_shape=jax.ShapeDtypeStruct(latents.shape...  83.5 us
    unnamed x2, local copies, waits for them, and re-layouts  4.35 us

commit v1 on v0

--- a/solution.py
+++ b/solution.py
@@ -210,10 +210,11 @@
 BAND = 32
 
 
-def turn_tables(tokens):
+def turn_tables(blocks, own):
     freq_count = ROTARY_DIM // 4
     inverse = 10000.0 ** (-np.arange(freq_count) / freq_count)
-    position = np.arange(tokens)
+    tokens = blocks * 4 * own
+    position = np.arange(tokens).reshape(blocks, 4, 2, own // 2).swapaxes(1, 2).reshape(-1)
     cosine = np.zeros((tokens, 128), np.float32)
     sine = np.zeros((tokens, 128), np.float32)
     cosine[:, :PLAIN_QK_DIM] = 1.0
@@ -241,11 +242,11 @@
 
 
 def block_kernel(
-    cond_ref,
-    bias_ref,
-    qgain_ref,
-    kvgain_ref,
-    rope_ref,
+    cond_hbm,
+    bias_hbm,
+    qgain_hbm,
+    kvgain_hbm,
+    rope_hbm,
     lat_hbm,
     ctx_hbm,
     wsh_hbm,
@@ -259,7 +260,12 @@
     wo_hbm,
     cos_hbm,
     sin_hbm,
-    out_ref,
+    out_hbm,
+    cond_ref,
+    bias_ref,
+    qgain_ref,
+    kvgain_ref,
+    rope_ref,
     cond16,
     w3,
     lat,
@@ -270,10 +276,10 @@
     modp,
     mod,
     cq,
-    kv,
-    kvc,
+    kvx,
+    krx,
     kraw,
-    ck,
+    ckn,
     cqn,
     wqu,
     wku,
@@ -291,14 +297,17 @@
     pr,
     st_mean,
     st_rate,
-    part,
+    part_self,
+    part_other,
+    outv,
     load_sem,
     send_sem,
     recv_sem,
     zsend,
     zrecv,
-    dsend,
-    drecv,
+    ssend,
+    srecv,
+    out_sem,
 ):
     f32, bf16 = jnp.float32, jnp.bfloat16
     spn = lax.axis_size("sp")
@@ -309,16 +318,16 @@
     p1, p2, p3 = p ^ 1, p ^ 2, p ^ 3
     own = lat.shape[1]
     width = lat.shape[2]
+    half = own // 2
     tok = own * 4
     pair = own * 2
     ctxn = ctx.shape[0]
     seg = tok + ctxn
+    arows = ctxn + pair
     modw = w3.shape[2]
     heads = qh.shape[0]
-    hrow = seg // 2
-    qcols = cq.shape[3]
-    kcols = kv.shape[3]
-    krank = 4 * kcols
+    kcols = kvx.shape[3]
+    spans = ((0, arows), (arows, pair))
 
     loads = []
 
@@ -329,6 +338,8 @@
         return copy
 
     l_lat = load(lat_hbm, lat.at[p])
+    l_cond = load(cond_hbm, cond_ref)
+    l_rope = load(rope_hbm, rope_ref)
     l_w3 = [load(ref, w3.at[i]) for i, ref in enumerate((wsh_hbm, wsc_hbm, wga_hbm))]
     l_ctx = load(ctx_hbm, ctx)
     l_kd = load(wkd_hbm, wkvr.at[:, pl.ds(0, kcols)])
@@ -340,6 +351,11 @@
     l_vu = load(wvu_hbm, wvu)
     l_qu = load(wqu_hbm, wqu)
     l_wo = load(wo_hbm, wo)
+    l_small = [
+        load(bias_hbm, bias_ref),
+        load(qgain_hbm, qgain_ref),
+        load(kvgain_hbm, kvgain_ref),
+    ]
 
     barrier = pltpu.get_barrier_semaphore()
     for peer in (p1, p2, p3):
@@ -351,18 +367,18 @@
 
     sends = []
 
-    def remote(src, dst, index, target):
+    def copy_to(src, dst, s_sem, r_sem, target):
         return pltpu.make_async_remote_copy(
             src_ref=src,
             dst_ref=dst,
-            send_sem=send_sem.at[index],
-            recv_sem=recv_sem.at[index],
+            send_sem=s_sem,
+            recv_sem=r_sem,
             device_id=target,
             device_id_type=MESH,
         )
 
     def send(src, dst, index, target):
-        copy = remote(src, dst, index, target)
+        copy = copy_to(src, dst, send_sem.at[index], recv_sem.at[index], target)
         copy.start()
         sends.append(copy)
         return copy
@@ -373,43 +389,46 @@
         counter[0] += 1
         return counter[0] - 1
 
-    def spread(view, far_view=None):
+    def near(view):
+        return send(view(p), view(p), fresh(), {"tp": p1}).wait_recv
+
+    def far(view, far_view=None):
         far_view = far_view or view
-        i1, i2, i3 = fresh(), fresh(), fresh()
+        i2, i3 = fresh(), fresh()
         first = send(view(p), view(p), i2, {"tp": p2})
-        second = send(view(p), view(p), i1, {"tp": p1})
 
         def relay():
             first.wait_recv()
-            third = send(far_view(p2), far_view(p2), i3, {"tp": p1})
-            return third.wait_recv
-
-        return relay, second.wait_recv
-
+            return send(far_view(p2), far_view(p2), i3, {"tp": p1}).wait_recv
+
+        return relay
+
+    l_cond.wait()
     cond16[...] = jnp.zeros_like(cond16)
     cond16[0:2, :] = cond_ref[...]
     conditions = cond16[...]
     act = (conditions / (1.0 + jnp.exp(-conditions))).astype(bf16)
+    l_rope.wait()
+    for c in range(0, width, 128):
+        wkvr[c : c + 128, kcols:] = jnp.concatenate(
+            [
+                jnp.swapaxes(rope_ref[:, c : c + 128].astype(f32), 0, 1).astype(bf16),
+                jnp.zeros((128, wkvr.shape[1] - kcols - ROTARY_DIM), bf16),
+            ],
+            axis=1,
+        )
 
     pl.semaphore_wait(barrier, 3 + spn - 1)
-    def near(view):
-        return send(view(p), view(p), fresh(), {"tp": p1}).wait_recv
-
-    def far(view):
-        i2, i3 = fresh(), fresh()
-        first = send(view(p), view(p), i2, {"tp": p2})
-
-        def relay():
-            first.wait_recv()
-            return send(view(p2), view(p2), i3, {"tp": p1}).wait_recv
-
-        return relay
 
     l_lat.wait()
+    pieces_a = [(0, BAND), (BAND, half - BAND)]
+    pieces_b = [(half, BAND), (half + BAND, half - BAND)]
+
+    def piece_of(r, n):
+        return lambda slot: lat.at[slot, pl.ds(r, n)]
+
+    relay_lat = [far(piece_of(*pieces_a[0]))]
     lat_near = near(lambda slot: lat.at[slot])
-    lat_rows = [slice(r, r + BAND) for r in range(0, own, BAND)]
-    lat_views = [lambda slot, r=r: lat.at[slot, pl.ds(r.start, BAND)] for r in lat_rows]
-    lat_relay = [far(lat_views[0])]
 
     for i in range(3):
         l_w3[i].wait()
@@ -421,34 +440,32 @@
         mod_waits.append(
             send(modp.at[z], modp.at[z], fresh(), {"sp": lax.rem(z + d, spn)})
         )
-    wkvr[:, kcols + ROTARY_DIM :] = jnp.zeros((width, wkvr.shape[1] - kcols - ROTARY_DIM), bf16)
-    wkvr[:, kcols : kcols + ROTARY_DIM] = rope_ref[...]
-
-    def measured(src, row_count, dst_row):
-        @pl.loop(0, row_count // BAND)
+
+    def measured(src, row_count, dst_row, step=BAND):
+        @pl.loop(0, row_count // step)
         def _(i):
-            rows = pl.ds(pl.multiple_of(i * BAND, BAND), BAND)
-            to = pl.ds(pl.multiple_of(dst_row + i * BAND, BAND), BAND)
+            rows = pl.ds(pl.multiple_of(i * step, STEP), step)
+            to = pl.ds(pl.multiple_of(dst_row + i * step, STEP), step)
             tiles = [slice(c, c + 128) for c in range(0, width, 128)]
-            sums = jnp.zeros((BAND, 128), f32)
+            sums = jnp.zeros((step, 128), f32)
             for c in tiles:
                 sums = sums + src[rows, c].astype(f32)
             mean = jnp.broadcast_to(
-                jnp.sum(sums, axis=-1, keepdims=True) * (1.0 / width), (BAND, 128)
+                jnp.sum(sums, axis=-1, keepdims=True) * (1.0 / width), (step, 128)
             )
-            squares = jnp.zeros((BAND, 128), f32)
+            squares = jnp.zeros((step, 128), f32)
             for c in tiles:
                 center = src[rows, c].astype(f32) - mean
                 squares = squares + center * center
             spread_of = jnp.sum(squares, axis=-1, keepdims=True) * (1.0 / width)
             st_mean[to, :] = mean
-            st_rate[to, :] = jnp.broadcast_to(lax.rsqrt(spread_of + EPSILON), (BAND, 128))
-
-    def modulate(src, row_count, dst_row, which):
-        @pl.loop(0, row_count // BAND)
+            st_rate[to, :] = jnp.broadcast_to(lax.rsqrt(spread_of + EPSILON), (step, 128))
+
+    def modulate(src, row_count, dst_row, which, step=BAND):
+        @pl.loop(0, row_count // step)
         def _(i):
-            rows = pl.ds(pl.multiple_of(i * BAND, BAND), BAND)
-            to = pl.ds(pl.multiple_of(dst_row + i * BAND, BAND), BAND)
+            rows = pl.ds(pl.multiple_of(i * step, STEP), step)
+            to = pl.ds(pl.multiple_of(dst_row + i * step, STEP), step)
             mean, rate = st_mean[to, :], st_rate[to, :]
             for c in range(0, width, 128):
                 j, k = c // modw, c % modw
@@ -457,9 +474,21 @@
                 normed = (src[rows, c : c + 128].astype(f32) - mean) * rate
                 hid[to, c : c + 128] = (normed * (1.0 + scale_by) + shift_by).astype(bf16)
 
-    measured(lat.at[p], own, p * own)
+    def hid_row(dev, r):
+        return ctxn + (r // half) * pair + dev * half + r % half
+
+    def band_view(dev, b):
+        return lat.at[dev, pl.ds(b * half, half)]
+
+    def take(dev, piece):
+        r, n = piece
+        measured(lat.at[dev, pl.ds(r, n)], n, hid_row(dev, r), n)
+        modulate(lat.at[dev, pl.ds(r, n)], n, hid_row(dev, r), 0, n)
+
+    for b in range(2):
+        measured(band_view(p, b), half, hid_row(p, b * half), STEP)
     l_ctx.wait()
-    measured(ctx, ctxn, tok)
+    measured(ctx, ctxn, 0)
     for copy in mod_waits:
         copy.wait_recv()
     total = modp[0]
@@ -467,69 +496,160 @@
         total = total + modp[i]
     mod[p] = total
     mod_waits = [send(mod.at[p], mod.at[p], fresh(), {"tp": peer}) for peer in (p2, p3, p1)]
-    for view in lat_views[1:]:
-        lat_relay.append(far(view))
+    for piece in pieces_a[1:] + pieces_b:
+        relay_lat.append(far(piece_of(*piece)))
     lat_near()
-    measured(lat.at[p1], own, p1 * own)
-    lat_far = [lat_relay[0]()]
+    for b in range(2):
+        measured(band_view(p1, b), half, hid_row(p1, b * half), STEP)
+    lat_far = [relay_lat[0]()]
     for copy in mod_waits:
         copy.wait_recv()
-
-    modulate(ctx, ctxn, tok, 1)
+    modulate(ctx, ctxn, 0, 1)
+    for dev in (p, p1):
+        modulate(band_view(dev, 0), half, hid_row(dev, 0), 0, STEP)
+    take(p2, pieces_a[0])
+    lat_far.append(relay_lat[1]())
+    take(p2, pieces_a[1])
+    for n, piece in enumerate(pieces_a):
+        lat_far[n]()
+        take(p3, piece)
+
+    def kv_piece(o, slot, part):
+        first, count = spans[part]
+        return kvx.at[o, slot, pl.ds(first, count)]
+
+    def kr_piece(o, part):
+        first, count = spans[part]
+        return krx.at[o, pl.ds(first // 4, count // 4)]
+
+    class Hop:
+        def __init__(self, origin, target, way, part):
+            views = (kv_piece(origin, p, part), kr_piece(origin, part))
+            self.copies = [
+                copy_to(
+                    view,
+                    view,
+                    zsend.at[way, part, kind, origin],
+                    zrecv.at[part, kind, origin],
+                    {"sp": target},
+                )
+                for kind, view in enumerate(views)
+            ]
+
+        def start(self):
+            for copy in self.copies:
+                copy.start()
+
+        def wait_recv(self):
+            for copy in self.copies:
+                copy.wait_recv()
+
+        def wait_send(self):
+            for copy in self.copies:
+                copy.wait_send()
+
+    def swap(o, part, kind):
+        view = kv_piece(o, p2 if kind == 2 else p, part)
+        target = p2 if kind == 0 else p1
+        return copy_to(
+            view, view, ssend.at[kind, part, o], srecv.at[kind, part, o], {"tp": target}
+        )
+
+    has_right = z + 1 < spn
+    has_left = z >= 1
+
+    def spread(o, part):
+        swap(o, part, 0).start()
+        swap(o, part, 1).start()
+
+    def relay(o, part):
+        swap(o, part, 0).wait_recv()
+        swap(o, part, 2).start()
+
+    def gathered(o, part):
+        swap(o, part, 1).wait_recv()
+        swap(o, part, 2).wait_recv()
+
+    def at_distance(step, fn):
+        left, right = z - 1 - step, z + 1 + step
+
+        @pl.when(left >= 0)
+        def _():
+            fn(left, 0, z + 1, has_right)
+
+        @pl.when(right < spn)
+        def _():
+            fn(right, 1, z - 1, has_left)
+
+    def forward(step, part):
+        def one(o, way, onward, more):
+            Hop(o, z, way, part).wait_recv()
+
+            @pl.when(more)
+            def _():
+                Hop(o, onward, way, part).start()
+
+        at_distance(step, one)
+
+    def spread_at(step, part):
+        at_distance(step, lambda o, way, onward, more: spread(o, part))
+
+    def down(part):
+        first, count = spans[part]
+        both = jnp.dot(hid[first : first + count, :], wkvr[...], preferred_element_type=f32)
+        kvx[z, p, first : first + count, :] = both[:, :kcols].astype(bf16)
+        kraw[first : first + count, :] = pltpu.roll(both[:, kcols:], 64, 1)
+        low = max(first, ctxn)
+        tabled = slice(low - ctxn, first + count - ctxn)
+        kraw[low : first + count, :] = turned(
+            kraw[low : first + count, :], cosv[tabled, :], sinv[tabled, :]
+        )
+        for t in range(first // 64, (first + count) // 64):
+            packed = None
+            for j in range(4):
+                row = 64 * t + j * STEP
+                moved = pltpu.roll(kraw[row : row + STEP, :], (32 * j + 64) % 128, 1)
+                packed = moved if packed is None else packed + moved
+            krx[z, STEP * t : STEP * t + STEP, :] = packed.astype(bf16)
+        spread(z, part)
+
+        @pl.when(has_right)
+        def _():
+            Hop(z, z + 1, 0, part).start()
+
+        @pl.when(has_left)
+        def _():
+            Hop(z, z - 1, 1, part).start()
+
+        rows = slice(low, first + count)
+        cq[p, part] = jnp.dot(hid[rows, :], wqd[...], preferred_element_type=f32).astype(bf16)
+        view = lambda slot: cq.at[slot, part]
+        return far(view), near(view)
+
     l_kd.wait()
     l_qd.wait()
-    mixed_ctx = jnp.dot(hid[tok:, :], wkvr[...], preferred_element_type=f32)
-    kvc[p] = mixed_ctx[:, :kcols].astype(bf16)
-    kraw[tok:, :] = mixed_ctx[:, kcols:]
-    relays = [spread(lambda slot: kvc.at[slot])]
-
-    modulate(lat.at[p], own, p * own, 0)
-    modulate(lat.at[p1], own, p1 * own, 0)
-
-    def down(half):
-        rows = pl.ds(pl.multiple_of(half * pair, STEP), pair)
-        both = jnp.dot(hid[rows, :], wkvr[...], preferred_element_type=f32)
-        kv[p, half] = both[:, :kcols].astype(bf16)
-        kraw[rows, :] = both[:, kcols:]
-        one = spread(lambda slot: kv.at[slot, half], lambda slot: kv.at[slot, 1 - half])
-        cq[p, half] = jnp.dot(hid[rows, :], wqd[...], preferred_element_type=f32).astype(bf16)
-        return one, spread(lambda slot: cq.at[slot, half], lambda slot: cq.at[slot, 1 - half])
-
-    kv_a, cq_a = down(side)
-    for n, r in enumerate(lat_rows):
-        if n:
-            lat_far.append(lat_relay[n]())
-        piece = lat.at[p2, pl.ds(r.start, BAND)]
-        measured(piece, BAND, p2 * own + r.start)
-        modulate(piece, BAND, p2 * own + r.start, 0)
-    for n, r in enumerate(lat_rows):
-        lat_far[n]()
-        piece = lat.at[p3, pl.ds(r.start, BAND)]
-        measured(piece, BAND, p3 * own + r.start)
-        modulate(piece, BAND, p3 * own + r.start, 0)
-    kv_b, cq_b = down(1 - side)
-    relays += [kv_a, kv_b]
-    kv_far = [r() for r, _ in relays]
-    for w in kv_far:
-        w()
-    for _, w in relays:
-        w()
-
     l_cos.wait()
     l_sin.wait()
-    kr_lat = turned(pltpu.roll(kraw[:tok, :], 64, 1), cosv[...], sinv[...])
-    kraw[:tok, :] = kr_lat
-    kraw[tok:, :] = pltpu.roll(kraw[tok:, :], 64, 1)
-    for hf in range(2):
-        for t in range(4):
-            packed = None
-            for j in range(4):
-                first_row = hf * hrow + (4 * t + j) * STEP
-                moved = pltpu.roll(
-                    kraw[first_row : first_row + STEP, :], (32 * j + 64) % 128, 1
-                )
-                packed = moved if packed is None else packed + moved
-            ck[z, hf, hrow : hrow + STEP, 128 * t : 128 * t + 128] = packed.astype(bf16)
+    cq_a = down(0)
+    for dev in (p, p1):
+        modulate(band_view(dev, 1), half, hid_row(dev, half), 0, STEP)
+    for n, piece in enumerate(pieces_b):
+        lat_far.append(relay_lat[2 + n]())
+        take(p2, piece)
+    forward(0, 0)
+    for n, piece in enumerate(pieces_b):
+        lat_far[2 + n]()
+        take(p3, piece)
+    relay(z, 0)
+    forward(1, 0)
+    cq_b = down(1)
+    spread_at(0, 0)
+    cq_waits = [cq_a[1], cq_b[1], cq_a[0]()]
+    forward(0, 1)
+    spread_at(0, 1)
+    relay(z, 1)
+    forward(2, 0)
+    spread_at(1, 0)
 
     def rms(pieces, gain_ref, store):
         values = [piece.astype(f32) for piece in pieces]
@@ -543,113 +663,23 @@
             gain = gain_ref[0:1, j * cols : (j + 1) * cols]
             store(slice(j * cols, (j + 1) * cols), (v * factor * gain).astype(bf16))
 
-    for piece in range(seg // 64):
-        base = piece * 64
-        if base < tok:
-            chunk = [kv[r, base // pair, base % pair : base % pair + 64, :] for r in range(4)]
-        else:
-            chunk = [kvc[r, base - tok : base - tok + 64, :] for r in range(4)]
-
-        def put(cols, value, base=base):
-            ck[z, base // hrow, base % hrow : base % hrow + 64, cols] = value
-
-        rms(chunk, kvgain_ref, put)
-
-    def hop(origin, target, way):
-        return pltpu.make_async_remote_copy(
-            src_ref=ck.at[origin, core],
-            dst_ref=ck.at[origin, core],
-            send_sem=zsend.at[way, origin],
-            recv_sem=zrecv.at[origin],
-            device_id={"sp": target},
-            device_id_type=MESH,
-        )
-
-    def cross(origin, half):
-        return pltpu.make_async_remote_copy(
-            src_ref=ck.at[origin, half],
-            dst_ref=ck.at[origin, half],
-            send_sem=dsend.at[origin],
-            recv_sem=drecv.at[origin],
-            device_id={"tp": p1},
-            device_id_type=MESH,
-        )
-
-    has_right = z + 1 < spn
-    has_left = z >= 1
-
-    @pl.when(has_right)
-    def _():
-        hop(z, z + 1, 0).start()
-
-    @pl.when(has_left)
-    def _():
-        hop(z, z - 1, 1).start()
-
-    w_cq = [cq_a[0](), cq_b[0]()]
-    for w in w_cq:
-        w()
-    cq_a[1]()
-    cq_b[1]()
-    for piece in range(tok // 64):
-        base = piece * 64
-        chunk = [cq[r, base // pair, base % pair : base % pair + 64, :] for r in range(4)]
-
-        def put(cols, value, base=base):
-            cqn[base : base + 64, cols] = value
-
-        rms(chunk, qgain_ref, put)
-    l_qu.wait()
-    q_all = jnp.dot(cqn[...], wqu[...], preferred_element_type=f32)
-    lane = lanes_of((tok, 128))
-    for h in range(heads):
-        offset = h * (PLAIN_QK_DIM + ROTARY_DIM)
-        tile, shift = offset // 128, offset % 128
-        head = q_all[:, 128 * tile : 128 * tile + 128]
-        if shift:
-            head = pltpu.roll(head, 128 - shift, 1)
-            if shift + PLAIN_QK_DIM + ROTARY_DIM > 128:
-                rest = pltpu.roll(q_all[:, 128 * tile + 128 : 128 * tile + 256], 128 - shift, 1)
-                head = jnp.where(lane < 128 - shift, head, rest)
-        qh[h] = turned(head, cosv[...], sinv[...]).astype(bf16)
-    l_ku.wait()
-    l_vu.wait()
-    acc[...] = jnp.zeros_like(acc)
-    mx[...] = jnp.full(mx.shape, NEGATIVE, f32)
-    factor = (PLAIN_QK_DIM + ROTARY_DIM) ** (-0.5) * LOG2E
-
-    def arrive(step):
-        left, right = z - 1 - step, z + 1 + step
-
-        @pl.when(left >= 0)
-        def _():
-            hop(left, z, 0).wait_recv()
-            cross(left, core).start()
-
-            @pl.when(has_right)
-            def _():
-                hop(left, z + 1, 0).start()
-
-        @pl.when(right < spn)
-        def _():
-            hop(right, z, 1).wait_recv()
-            cross(right, core).start()
-
-            @pl.when(has_left)
-            def _():
-                hop(right, z - 1, 1).start()
-
     def expand(block):
+        for base in range(0, seg, 64):
+            def put(cols, value, base=base):
+                ckn[base : base + 64, cols] = value
+
+            rms([kvx[block, r, base : base + 64, :] for r in range(4)], kvgain_ref, put)
+        hrow = seg // 2
         lane_h = lanes_of((hrow, 128))
         ones = (lane_h == VALUE_DIM).astype(f32)
         lane_s = lanes_of((STEP, 128))
         on_rope = (lane_s >= PLAIN_QK_DIM) & (lane_s < PLAIN_QK_DIM + ROTARY_DIM)
         for hf in range(2):
             rows = slice(hf * hrow, (hf + 1) * hrow)
-            latent_rows = ck[block, hf, :hrow, :]
+            latent_rows = ckn[rows, :]
             pieces = []
-            for t in range(4):
-                packed = ck[block, hf, hrow : hrow + STEP, 128 * t : 128 * t + 128].astype(f32)
+            for t in range(4 * hf, 4 * hf + 4):
+                packed = krx[block, STEP * t : STEP * t + STEP, :].astype(f32)
                 for j in range(4):
                     moved = pltpu.roll(packed, (192 - 32 * j) % 128, 1)
                     pieces.append(jnp.where(on_rope, moved, 0.0))
@@ -668,6 +698,48 @@
                     lane_h < 64, pltpu.roll(v2, 64, 1), ones
                 ).astype(bf16)
 
+    for copy in l_small:
+        copy.wait()
+    l_ku.wait()
+    l_vu.wait()
+    for part in range(2):
+        gathered(z, part)
+    forward(1, 1)
+    spread_at(1, 1)
+    cq_waits.append(cq_b[0]())
+    spread_at(2, 0)
+    expand(z)
+    acc[...] = jnp.zeros_like(acc)
+    mx[...] = jnp.full(mx.shape, NEGATIVE, f32)
+    factor = (PLAIN_QK_DIM + ROTARY_DIM) ** (-0.5) * LOG2E
+
+    for w in cq_waits:
+        w()
+    for base in range(0, tok, 64):
+        def put(cols, value, base=base):
+            cqn[base : base + 64, cols] = value
+
+        rms(
+            [cq[r, base // pair, base % pair : base % pair + 64, :] for r in range(4)],
+            qgain_ref,
+            put,
+        )
+    l_qu.wait()
+    q_all = jnp.dot(cqn[...], wqu[...], preferred_element_type=f32)
+    lane = lanes_of((tok, 128))
+    for h in range(heads):
+        offset = h * (PLAIN_QK_DIM + ROTARY_DIM)
+        tile, shift = offset // 128, offset % 128
+        head = q_all[:, 128 * tile : 128 * tile + 128]
+        if shift:
+            head = pltpu.roll(head, 128 - shift, 1)
+            if shift + PLAIN_QK_DIM + ROTARY_DIM > 128:
+                rest = pltpu.roll(q_all[:, 128 * tile + 128 : 128 * tile + 256], 128 - shift, 1)
+                head = jnp.where(lane < 128 - shift, head, rest)
+        qh[h] = turned(head, cosv[...], sinv[...]).astype(bf16)
+    forward(2, 1)
+    spread_at(2, 1)
+
     def score(h):
         return lax.dot_general(
             qh[h], kb[h], (((1,), (1,)), ((), ())), preferred_element_type=f32
@@ -676,7 +748,7 @@
     def attend(h, scores):
         tiles = [scores[:, c : c + 128] * factor for c in range(0, seg, 128)]
         bias = bias_ref[h] * LOG2E
-        tiles = [t + bias if n * 128 >= tok else t for n, t in enumerate(tiles)]
+        tiles = [t + bias if n * 128 < ctxn else t for n, t in enumerate(tiles)]
         best = functools.reduce(jnp.maximum, tiles)
         old = mx[h]
         new = jnp.maximum(old, jnp.max(best, axis=-1, keepdims=True))
@@ -696,27 +768,31 @@
 
     def block_at(step):
         below = jnp.minimum(z, spn - 1 - z)
-        near = jnp.where(lax.rem(step, 2) == 1, z - (step + 1) // 2, z + step // 2)
+        near_block = jnp.where(lax.rem(step, 2) == 1, z - (step + 1) // 2, z + step // 2)
         past = jnp.where(z < spn - 1 - z, step, spn - 1 - step)
-        return jnp.where(step <= 2 * below, near, past)
-
-    @pl.loop(0, spn - 1)
+        return jnp.where(step <= 2 * below, near_block, past)
+
+    relay(block_at(jnp.int32(1)), 0)
+    relay(block_at(jnp.int32(1)), 1)
+
+    @pl.loop(1, spn)
     def _(step):
-        @pl.when(step > 0)
+        attend_all(lambda h: None)
+        block = block_at(step)
+
+        @pl.when(step + 1 < spn)
         def _():
-            arrive(step - 1)
-
-        block = block_at(step)
-
-        @pl.when(step > 0)
-        def _():
-            cross(block, 1 - core).wait_recv()
-
+            later = block_at(step + 1)
+            relay(later, 0)
+            relay(later, 1)
+
+        for part in range(2):
+            gathered(block, part)
         expand(block)
-        attend_all(lambda h: None)
 
     att_relay, att_near = [], []
     lane64 = lane < 64
+    quarter = own
 
     def finish(h):
         if h % 2 == 0:
@@ -726,86 +802,121 @@
         for g in (h - 1, h):
             a = acc[g]
             outs.append(a / a[:, VALUE_DIM : VALUE_DIM + 1])
-        att[p, hp] = jnp.where(lane64, outs[0], pltpu.roll(outs[1], 64, 1)).astype(bf16)
-        att_relay.append(far(lambda slot: att.at[slot, hp]))
+        value = jnp.where(lane64, outs[0], pltpu.roll(outs[1], 64, 1)).astype(bf16)
+        for b in range(2):
+            for s in range(2):
+                row = (2 * b + s) * quarter
+                att[p, hp, b, s] = value[row : row + quarter]
+        att_relay.append(
+            far(
+                lambda slot: att.at[slot, hp, :, side],
+                lambda slot: att.at[slot, hp, :, 1 - side],
+            )
+        )
         att_near.append(near(lambda slot: att.at[slot, hp]))
 
-    arrive(spn - 2)
-    last_block = block_at(jnp.int32(spn - 1))
-    cross(last_block, 1 - core).wait_recv()
-    expand(last_block)
     attend_all(finish)
 
+    hps = heads // 2
+    for first in range(0, hps, 2):
+        att_relay.append(
+            far(
+                lambda slot, first=first: att.at[slot, pl.ds(first, 2), :, 1 - side],
+                lambda slot, first=first: att.at[slot, pl.ds(first, 2), :, side],
+            )
+        )
     l_wo.wait()
     half_k = heads * VALUE_DIM * 2
-    order = (p2, p3, p1, p)
-
-    def project(dest, chip):
-        rows = pl.ds(pl.multiple_of(dest * own, STEP), own)
+
+    def project(rows_side, chip):
         joined = jnp.concatenate(
-            [att[2 * chip + r, hp, rows, :] for r in range(2) for hp in range(heads // 2)], axis=1
+            [
+                jnp.concatenate([att[2 * chip + r, hp, b, rows_side] for b in range(2)], axis=0)
+                for r in range(2)
+                for hp in range(hps)
+            ],
+            axis=1,
         )
         k_rows = pl.ds(pl.multiple_of(chip * half_k, 128), half_k)
         return jnp.dot(joined, wo[k_rows, :], preferred_element_type=f32)
 
-    att_far = [att_relay[0](), att_relay[1]()]
     for w in att_near:
         w()
-    for dest in order:
-        part[dest] = project(dest, side)
-    att_far += [r() for r in att_relay[2:]]
+    part_other[...] = project(1 - side, side)
+    att_far = [r() for r in att_relay[:2]]
+    part_self[...] = project(side, side)
+    att_far += [r() for r in att_relay[2:hps]]
     for w in att_far:
         w()
-    final = []
-    for dest in order:
-        made = (part[dest] + project(dest, 1 - side)).astype(bf16)
-        if dest is p:
-            pr[p] = made
-        else:
-            po[dest] = made
-            final.append(send(po.at[dest], pr.at[p], fresh(), {"tp": dest}))
-    for copy in final:
-        copy.wait_recv()
-
-    @pl.loop(0, own // STEP)
-    def _(i):
-        rows = pl.ds(pl.multiple_of(i * STEP, STEP), STEP)
-        for j in range(4):
-            cols = slice(j * modw, (j + 1) * modw)
-            gate = mod[j, 4:5, :]
-            out_ref[rows, cols] = (
-                lat[p, rows, cols].astype(f32) + gate * pr[j, rows, :].astype(f32)
+    made = (part_other[...] + project(1 - side, 1 - side)).astype(bf16)
+    for k in range(2):
+        for b in range(2):
+            row = b * own + k * half
+            po[k, b * half : (b + 1) * half, :] = made[row : row + half]
+    final = [
+        send(po.at[core], pr.at[p], fresh(), {"tp": p2}),
+        send(po.at[1 - core], pr.at[p], fresh(), {"tp": p3}),
+    ]
+    att_far = [r() for r in att_relay[hps:]]
+    for w in att_far:
+        w()
+    made = (part_self[...] + project(side, 1 - side)).astype(bf16)
+    for k in range(2):
+        for b in range(2):
+            row = b * own + k * half
+            po[2 + k, b * half : (b + 1) * half, :] = made[row : row + half]
+    close = send(po.at[2 + 1 - core], pr.at[p], fresh(), {"tp": p1})
+
+    stores = []
+
+    def mix(j, source):
+        cols = pl.ds(pl.multiple_of(j * modw, 128), modw)
+        gate = mod[j, 4:5, :]
+        for r in range(0, own, STEP):
+            outv[r : r + STEP, cols] = (
+                lat[p, r : r + STEP, cols].astype(f32)
+                + gate * source[r : r + STEP, :].astype(f32)
             ).astype(bf16)
+        copy = pltpu.make_async_copy(
+            outv.at[:, cols], out_hbm.at[:, cols], out_sem.at[len(stores)]
+        )
+        copy.start()
+        stores.append(copy)
+
+    mix(p, po.at[2 + core])
+    close.wait_recv()
+    mix(p1, pr.at[p1])
+    final[0].wait_recv()
+    mix(p2, pr.at[p2])
+    final[1].wait_recv()
+    mix(p3, pr.at[p3])
 
     for copy in sends:
         copy.wait_send()
-
-    @pl.when(has_right)
-    def _():
-        hop(z, z + 1, 0).wait_send()
-
-    @pl.when(has_left)
-    def _():
-        hop(z, z - 1, 1).wait_send()
-
-    for step in range(spn - 1):
-        left, right = z - 1 - step, z + 1 + step
-
-        @pl.when(left >= 0)
+    for part in range(2):
+        for kind in range(3):
+            swap(z, part, kind).wait_send()
+
+        @pl.when(has_right)
         def _():
-            cross(left, core).wait_send()
-
-            @pl.when(has_right)
+            Hop(z, z + 1, 0, part).wait_send()
+
+        @pl.when(has_left)
+        def _():
+            Hop(z, z - 1, 1, part).wait_send()
+
+        def drain(o, way, onward, more):
+            for kind in range(3):
+                swap(o, part, kind).wait_send()
+
+            @pl.when(more)
             def _():
-                hop(left, z + 1, 0).wait_send()
-
-        @pl.when(right < spn)
-        def _():
-            cross(right, core).wait_send()
-
-            @pl.when(has_left)
-            def _():
-                hop(right, z - 1, 1).wait_send()
+                Hop(o, onward, way, part).wait_send()
+
+        for step in range(spn - 1):
+            at_distance(step, drain)
+    for copy in stores:
+        copy.wait()
 
 
 def fused_device(
@@ -836,12 +947,15 @@
     modw = w_shift.shape[1]
     kdim, qcols = w_qdown.shape
     kcols = w_kvdown.shape[1]
-    cosine, sine = turn_tables(tok * spn)
-    vmem = pl.BlockSpec(memory_space=pltpu.VMEM)
-    smem = pl.BlockSpec(memory_space=pltpu.SMEM)
-    hbm = pl.BlockSpec(memory_space=pl.ANY)
+    cosine, sine = turn_tables(spn, own)
+    hbm = pl.BlockSpec(memory_space=pltpu.HBM)
     V, DMA = pltpu.VMEM, pltpu.SemaphoreType.DMA
     scratch = [
+        V(conditions.shape, f32),
+        pltpu.SMEM(context_bias.shape, f32),
+        V((1,) + q_gain.shape, f32),
+        V((1,) + latent_norm_gain.shape, f32),
+        V(w_rope.shape[::-1], bf16),
         V((16, conditions.shape[1]), f32),
         V((3,) + w_shift.shape, bf16),
         V((4, own, width), bf16),
@@ -852,10 +966,10 @@
         V((spn, 8, modw), f32),
         V((4, 8, modw), f32),
         V((4, 2, 2 * own, qcols), bf16),
-        V((4, 2, 2 * own, kcols), bf16),
-        V((4, ctxn, kcols), bf16),
+        V((spn, 4, seg, kcols), bf16),
+        V((spn, seg // 4, 128), bf16),
         V((seg, 128), f32),
-        V((spn, 2, seg // 2 + STEP, 4 * kcols), bf16),
+        V((seg, 4 * kcols), bf16),
         V((tok, 4 * qcols), bf16),
         V(query_up_weight.shape, bf16),
         V(key_up_weight.shape, bf16),
@@ -868,35 +982,38 @@
         V((heads, seg, 128), bf16),
         V((heads, tok, 128), f32),
         V((heads, tok, 128), f32),
-        V((4, heads // 2, tok, 128), bf16),
+        V((4, heads // 2, 2, 2, own, 128), bf16),
         V((4, own, modw), bf16),
         V((4, own, modw), bf16),
         V((seg, 128), f32),
         V((seg, 128), f32),
-        V((4, own, modw), f32),
-        DMA((13,)),
+        V((2 * own, modw), f32),
+        V((2 * own, modw), f32),
+        V((own, width), bf16),
+        DMA((18,)),
         DMA((48,)),
         DMA((48,)),
-        DMA((2, spn)),
-        DMA((spn,)),
-        DMA((spn,)),
-        DMA((spn,)),
+        DMA((2, 2, 2, spn)),
+        DMA((2, 2, spn)),
+        DMA((3, 2, spn)),
+        DMA((3, 2, spn)),
+        DMA((4,)),
     ]
     return pl.pallas_call(
         block_kernel,
         out_shape=jax.ShapeDtypeStruct(latents.shape, bf16),
-        in_specs=[vmem, smem, vmem, vmem, vmem] + [hbm] * 13,
-        out_specs=vmem,
+        in_specs=[hbm] * 18,
+        out_specs=hbm,
         scratch_shapes=scratch,
         compiler_params=pltpu.CompilerParams(
-            collective_id=0, has_side_effects=True, vmem_limit_bytes=60 * 1024 * 1024
+            collective_id=0, has_side_effects=True, vmem_limit_bytes=56 * 1024 * 1024
         ),
     )(
         conditions,
         context_bias,
         q_gain[None, :],
         latent_norm_gain[None, :],
-        w_rope,
+        w_rope.T,
         latents,
         context,
         w_shift,
@@ -918,7 +1035,8 @@
     fits = (
         lax.axis_size("tp") == 4
         and latents.shape[0] % 32 == 0
-        and context.shape[0] % 64 == 0
+        and context.shape[0] % 128 == 0
+        and latents.shape[0] > 2 * BAND
         and (4 * latents.shape[0] + context.shape[0]) == 512
         and arrays[6].shape[1] == 256
         and arrays[7].shape[1] == 128

time: 88.2 us -> 75.5 us (0.86)
  Pallas kernels: 83.5 us -> 73.3 us
  local copies, waits for them, and re-layouts: 4.35 us -> 2.06 us
    pallas_call x1, Pallas kernels: 83.5 us -> 73.3 us  [fused_device(): pl.pallas_call(block_kernel, out_shape=jax.ShapeDtypeStruct(latents.shape...]
    unnamed x2 -> x1, local copies, waits for them, and re-layouts: 4.35 us -> 2.06 us
where the time goes in v1:
time: 75.5 us; the launch traced here: 75.3 us
  Pallas kernels  73.3 us (97%)
  local copies, waits for them, and re-layouts  2.06 us (3%)
    pallas_call x1, Pallas kernels, fused_device(): pl.pallas_call(block_kernel, out_shape=jax.ShapeDtypeStruct(latents.shape...  73.3 us
    unnamed x1, local copies, waits for them, and re-layouts  2.06 us

profile of v1, /device:TPU:0, one launch (start us, length us, event | category | flops | bytes accessed | tf_op | source)
XLA Modules:
  0.0 75.3 jit_solution(12457220058974374001)
XLA Ops:
  0.0 73.3 %shard_map.172 = bf16[96,4096]{1,0:T(8,128)(2,1)} custom-call(f32[2,1024]{1,0:T(2,128)} %cond_hbm.1, f32[8]{0:T(128)} %bias_hbm.1, f32[1,1024]{1,0:T(1,128)} %bitcast.4, f32[1,512]{1,0:T(1,128)} %bitcast.5, bf16[32,4096]{1,0:T(8,128)(2,1)} %bitcast.3, bf16[96,4096]{1,0:T(8,128)(2,1)} %lat_hbm.1, bf16[128,4096]{1,0:T(8,128)(2,1)} %ctx_hbm.1, ...), custom_call_target="tpu_custom_call" | custom-call | tf_op jit(solution)/shard_map/pallas_call | solution.py:1002
  73.3 2.1 %copy.20 = bf16[96,4096]{1,0:T(8,128)(2,1)} copy(bf16[96,4096]{1,0:T(8,128)(2,1)} %shard_map.172) | data formatting | bytes 1572864

commit v2 on v1

--- a/solution.py
+++ b/solution.py
@@ -208,6 +208,7 @@
 LOG2E = 1.4426950408889634
 STEP = 16
 BAND = 32
+RELAY_AFTER = 2
 
 
 def turn_tables(blocks, own):
@@ -260,7 +261,7 @@
     wo_hbm,
     cos_hbm,
     sin_hbm,
-    out_hbm,
+    out_ref,
     cond_ref,
     bias_ref,
     qgain_ref,
@@ -299,7 +300,6 @@
     st_rate,
     part_self,
     part_other,
-    outv,
     load_sem,
     send_sem,
     recv_sem,
@@ -307,7 +307,6 @@
     zrecv,
     ssend,
     srecv,
-    out_sem,
 ):
     f32, bf16 = jnp.float32, jnp.bfloat16
     spn = lax.axis_size("sp")
@@ -427,7 +426,7 @@
     def piece_of(r, n):
         return lambda slot: lat.at[slot, pl.ds(r, n)]
 
-    relay_lat = [far(piece_of(*pieces_a[0]))]
+    relay_lat = [far(piece_of(*piece)) for piece in pieces_a]
     lat_near = near(lambda slot: lat.at[slot])
 
     for i in range(3):
@@ -486,7 +485,7 @@
         modulate(lat.at[dev, pl.ds(r, n)], n, hid_row(dev, r), 0, n)
 
     for b in range(2):
-        measured(band_view(p, b), half, hid_row(p, b * half), STEP)
+        measured(band_view(p, b), half, hid_row(p, b * half), half)
     l_ctx.wait()
     measured(ctx, ctxn, 0)
     for copy in mod_waits:
@@ -495,18 +494,20 @@
     for i in range(1, spn):
         total = total + modp[i]
     mod[p] = total
-    mod_waits = [send(mod.at[p], mod.at[p], fresh(), {"tp": peer}) for peer in (p2, p3, p1)]
-    for piece in pieces_a[1:] + pieces_b:
+    mod_relay = far(lambda slot: mod.at[slot])
+    mod_near = near(lambda slot: mod.at[slot])
+    for piece in pieces_b:
         relay_lat.append(far(piece_of(*piece)))
     lat_near()
     for b in range(2):
-        measured(band_view(p1, b), half, hid_row(p1, b * half), STEP)
+        measured(band_view(p1, b), half, hid_row(p1, b * half), half)
     lat_far = [relay_lat[0]()]
-    for copy in mod_waits:
-        copy.wait_recv()
+    mod_far = mod_relay()
+    mod_near()
+    mod_far()
     modulate(ctx, ctxn, 0, 1)
     for dev in (p, p1):
-        modulate(band_view(dev, 0), half, hid_row(dev, 0), 0, STEP)
+        modulate(band_view(dev, 0), half, hid_row(dev, 0), 0, half)
     take(p2, pieces_a[0])
     lat_far.append(relay_lat[1]())
     take(p2, pieces_a[1])
@@ -591,10 +592,7 @@
 
         at_distance(step, one)
 
-    def spread_at(step, part):
-        at_distance(step, lambda o, way, onward, more: spread(o, part))
-
-    def down(part):
+    def down_kv(part):
         first, count = spans[part]
         both = jnp.dot(hid[first : first + count, :], wkvr[...], preferred_element_type=f32)
         kvx[z, p, first : first + count, :] = both[:, :kcols].astype(bf16)
@@ -621,7 +619,9 @@
         def _():
             Hop(z, z - 1, 1, part).start()
 
-        rows = slice(low, first + count)
+    def down_q(part):
+        first, count = spans[part]
+        rows = slice(max(first, ctxn), first + count)
         cq[p, part] = jnp.dot(hid[rows, :], wqd[...], preferred_element_type=f32).astype(bf16)
         view = lambda slot: cq.at[slot, part]
         return far(view), near(view)
@@ -630,9 +630,10 @@
     l_qd.wait()
     l_cos.wait()
     l_sin.wait()
-    cq_a = down(0)
+    down_kv(0)
+    cq_a = down_q(0)
     for dev in (p, p1):
-        modulate(band_view(dev, 1), half, hid_row(dev, half), 0, STEP)
+        modulate(band_view(dev, 1), half, hid_row(dev, half), 0, half)
     for n, piece in enumerate(pieces_b):
         lat_far.append(relay_lat[2 + n]())
         take(p2, piece)
@@ -640,16 +641,8 @@
     for n, piece in enumerate(pieces_b):
         lat_far[2 + n]()
         take(p3, piece)
-    relay(z, 0)
-    forward(1, 0)
-    cq_b = down(1)
-    spread_at(0, 0)
-    cq_waits = [cq_a[1], cq_b[1], cq_a[0]()]
-    forward(0, 1)
-    spread_at(0, 1)
-    relay(z, 1)
-    forward(2, 0)
-    spread_at(1, 0)
+    cq_b = down_q(1)
+    down_kv(1)
 
     def rms(pieces, gain_ref, store):
         values = [piece.astype(f32) for piece in pieces]
@@ -663,82 +656,98 @@
             gain = gain_ref[0:1, j * cols : (j + 1) * cols]
             store(slice(j * cols, (j + 1) * cols), (v * factor * gain).astype(bf16))
 
-    def expand(block):
-        for base in range(0, seg, 64):
+    def expand_half(block, hf):
+        hrow = seg // 2
+        for base in range(hf * hrow, (hf + 1) * hrow, 64):
             def put(cols, value, base=base):
                 ckn[base : base + 64, cols] = value
 
             rms([kvx[block, r, base : base + 64, :] for r in range(4)], kvgain_ref, put)
-        hrow = seg // 2
         lane_h = lanes_of((hrow, 128))
         ones = (lane_h == VALUE_DIM).astype(f32)
         lane_s = lanes_of((STEP, 128))
         on_rope = (lane_s >= PLAIN_QK_DIM) & (lane_s < PLAIN_QK_DIM + ROTARY_DIM)
-        for hf in range(2):
-            rows = slice(hf * hrow, (hf + 1) * hrow)
-            latent_rows = ckn[rows, :]
-            pieces = []
-            for t in range(4 * hf, 4 * hf + 4):
-                packed = krx[block, STEP * t : STEP * t + STEP, :].astype(f32)
-                for j in range(4):
-                    moved = pltpu.roll(packed, (192 - 32 * j) % 128, 1)
-                    pieces.append(jnp.where(on_rope, moved, 0.0))
-            rope_key = jnp.concatenate(pieces, axis=0)
-            keys = jnp.dot(latent_rows, wku[...], preferred_element_type=f32)
-            vals = jnp.dot(latent_rows, wvu[...], preferred_element_type=f32)
-            for hp in range(heads // 2):
-                cols = slice(128 * hp, 128 * hp + 128)
-                k2, v2 = keys[:, cols], vals[:, cols]
-                kb[2 * hp, rows, :] = jnp.where(lane_h < 64, k2, rope_key).astype(bf16)
-                kb[2 * hp + 1, rows, :] = jnp.where(
-                    lane_h < 64, pltpu.roll(k2, 64, 1), rope_key
-                ).astype(bf16)
-                vb[2 * hp, rows, :] = jnp.where(lane_h < 64, v2, ones).astype(bf16)
-                vb[2 * hp + 1, rows, :] = jnp.where(
-                    lane_h < 64, pltpu.roll(v2, 64, 1), ones
-                ).astype(bf16)
+        rows = slice(hf * hrow, (hf + 1) * hrow)
+        latent_rows = ckn[rows, :]
+        pieces = []
+        for t in range(4 * hf, 4 * hf + 4):
+            packed = krx[block, STEP * t : STEP * t + STEP, :].astype(f32)
+            for j in range(4):
+                moved = pltpu.roll(packed, (192 - 32 * j) % 128, 1)
+                pieces.append(jnp.where(on_rope, moved, 0.0))
+        rope_key = jnp.concatenate(pieces, axis=0)
+        keys = jnp.dot(latent_rows, wku[...], preferred_element_type=f32)
+        vals = jnp.dot(latent_rows, wvu[...], preferred_element_type=f32)
+        for hp in range(heads // 2):
+            cols = slice(128 * hp, 128 * hp + 128)
+            k2, v2 = keys[:, cols], vals[:, cols]
+            kb[2 * hp, rows, :] = jnp.where(lane_h < 64, k2, rope_key).astype(bf16)
+            kb[2 * hp + 1, rows, :] = jnp.where(
+                lane_h < 64, pltpu.roll(k2, 64, 1), rope_key
+            ).astype(bf16)
+            vb[2 * hp, rows, :] = jnp.where(lane_h < 64, v2, ones).astype(bf16)
+            vb[2 * hp + 1, rows, :] = jnp.where(
+                lane_h < 64, pltpu.roll(v2, 64, 1), ones
+            ).astype(bf16)
+
+    def block_at(step):
+        below = jnp.minimum(z, spn - 1 - z)
+        near_block = jnp.where(lax.rem(step, 2) == 1, z - (step + 1) // 2, z + step // 2)
+        past = jnp.where(z < spn - 1 - z, step, spn - 1 - step)
+        return jnp.where(step <= 2 * below, near_block, past)
+
+    lane = lanes_of((pair, 128))
+
+    def up_q(b):
+        for base in range(0, pair, 64):
+            def put(cols, value, base=base):
+                cqn[base : base + 64, cols] = value
+
+            rms([cq[r, b, base : base + 64, :] for r in range(4)], qgain_ref, put)
+        q_all = jnp.dot(cqn[...], wqu[...], preferred_element_type=f32)
+        rows = slice(b * pair, (b + 1) * pair)
+        for h in range(heads):
+            offset = h * (PLAIN_QK_DIM + ROTARY_DIM)
+            tile, shift = offset // 128, offset % 128
+            head = q_all[:, 128 * tile : 128 * tile + 128]
+            if shift:
+                head = pltpu.roll(head, 128 - shift, 1)
+                if shift + PLAIN_QK_DIM + ROTARY_DIM > 128:
+                    rest = q_all[:, 128 * tile + 128 : 128 * tile + 256]
+                    head = jnp.where(
+                        lane < 128 - shift, head, pltpu.roll(rest, 128 - shift, 1)
+                    )
+            qh[h, rows, :] = turned(head, cosv[rows, :], sinv[rows, :]).astype(bf16)
 
     for copy in l_small:
         copy.wait()
+    l_qu.wait()
     l_ku.wait()
     l_vu.wait()
-    for part in range(2):
-        gathered(z, part)
-    forward(1, 1)
-    spread_at(1, 1)
-    cq_waits.append(cq_b[0]())
-    spread_at(2, 0)
-    expand(z)
     acc[...] = jnp.zeros_like(acc)
     mx[...] = jnp.full(mx.shape, NEGATIVE, f32)
     factor = (PLAIN_QK_DIM + ROTARY_DIM) ** (-0.5) * LOG2E
-
+    blocks = [None] + [block_at(jnp.int32(step)) for step in range(1, spn)]
+
+    spread(blocks[1], 0)
+    cq_waits = [cq_a[1], cq_a[0]()]
+    relay(z, 0)
     for w in cq_waits:
         w()
-    for base in range(0, tok, 64):
-        def put(cols, value, base=base):
-            cqn[base : base + 64, cols] = value
-
-        rms(
-            [cq[r, base // pair, base % pair : base % pair + 64, :] for r in range(4)],
-            qgain_ref,
-            put,
-        )
-    l_qu.wait()
-    q_all = jnp.dot(cqn[...], wqu[...], preferred_element_type=f32)
-    lane = lanes_of((tok, 128))
-    for h in range(heads):
-        offset = h * (PLAIN_QK_DIM + ROTARY_DIM)
-        tile, shift = offset // 128, offset % 128
-        head = q_all[:, 128 * tile : 128 * tile + 128]
-        if shift:
-            head = pltpu.roll(head, 128 - shift, 1)
-            if shift + PLAIN_QK_DIM + ROTARY_DIM > 128:
-                rest = pltpu.roll(q_all[:, 128 * tile + 128 : 128 * tile + 256], 128 - shift, 1)
-                head = jnp.where(lane < 128 - shift, head, rest)
-        qh[h] = turned(head, cosv[...], sinv[...]).astype(bf16)
-    forward(2, 1)
-    spread_at(2, 1)
+    up_q(0)
+    forward(1, 0)
+    gathered(z, 0)
+    expand_half(z, 0)
+    cq_waits = [cq_b[1], cq_b[0]()]
+    relay(z, 1)
+    forward(0, 1)
+    spread(blocks[1], 1)
+    spread(blocks[2], 0)
+    for w in cq_waits:
+        w()
+    up_q(1)
+    gathered(z, 1)
+    expand_half(z, 1)
 
     def score(h):
         return lax.dot_general(
@@ -766,43 +775,48 @@
             after(h)
             scores = following
 
-    def block_at(step):
-        below = jnp.minimum(z, spn - 1 - z)
-        near_block = jnp.where(lax.rem(step, 2) == 1, z - (step + 1) // 2, z + step // 2)
-        past = jnp.where(z < spn - 1 - z, step, spn - 1 - step)
-        return jnp.where(step <= 2 * below, near_block, past)
-
-    relay(block_at(jnp.int32(1)), 0)
-    relay(block_at(jnp.int32(1)), 1)
-
     @pl.loop(1, spn)
     def _(step):
-        attend_all(lambda h: None)
         block = block_at(step)
 
-        @pl.when(step + 1 < spn)
-        def _():
-            later = block_at(step + 1)
-            relay(later, 0)
-            relay(later, 1)
-
+        def meanwhile(h):
+            if h != RELAY_AFTER:
+                return
+
+            @pl.when(step == 1)
+            def _():
+                forward(2, 0)
+                forward(1, 1)
+                spread(blocks[2], 1)
+                spread(blocks[3], 0)
+
+            for part in range(2):
+                relay(block, part)
+
+            @pl.when(step == 2)
+            def _():
+                forward(2, 1)
+                spread(blocks[3], 1)
+
+        attend_all(meanwhile)
         for part in range(2):
             gathered(block, part)
-        expand(block)
+        for hf in range(2):
+            expand_half(block, hf)
 
     att_relay, att_near = [], []
-    lane64 = lane < 64
+    lane64 = lanes_of((tok, 128)) < VALUE_DIM
     quarter = own
 
     def finish(h):
         if h % 2 == 0:
             return
         hp = h // 2
-        outs = []
-        for g in (h - 1, h):
-            a = acc[g]
-            outs.append(a / a[:, VALUE_DIM : VALUE_DIM + 1])
-        value = jnp.where(lane64, outs[0], pltpu.roll(outs[1], 64, 1)).astype(bf16)
+        low, high = acc[h - 1], acc[h]
+        totals = jnp.where(
+            lane64, low[:, VALUE_DIM : VALUE_DIM + 1], high[:, VALUE_DIM : VALUE_DIM + 1]
+        )
+        value = (jnp.where(lane64, low, pltpu.roll(high, 64, 1)) / totals).astype(bf16)
         for b in range(2):
             for s in range(2):
                 row = (2 * b + s) * quarter
@@ -867,21 +881,14 @@
             po[2 + k, b * half : (b + 1) * half, :] = made[row : row + half]
     close = send(po.at[2 + 1 - core], pr.at[p], fresh(), {"tp": p1})
 
-    stores = []
-
     def mix(j, source):
         cols = pl.ds(pl.multiple_of(j * modw, 128), modw)
         gate = mod[j, 4:5, :]
         for r in range(0, own, STEP):
-            outv[r : r + STEP, cols] = (
+            out_ref[r : r + STEP, cols] = (
                 lat[p, r : r + STEP, cols].astype(f32)
                 + gate * source[r : r + STEP, :].astype(f32)
             ).astype(bf16)
-        copy = pltpu.make_async_copy(
-            outv.at[:, cols], out_hbm.at[:, cols], out_sem.at[len(stores)]
-        )
-        copy.start()
-        stores.append(copy)
 
     mix(p, po.at[2 + core])
     close.wait_recv()
@@ -915,8 +922,6 @@
 
         for step in range(spn - 1):
             at_distance(step, drain)
-    for copy in stores:
-        copy.wait()
 
 
 def fused_device(
@@ -970,7 +975,7 @@
         V((spn, seg // 4, 128), bf16),
         V((seg, 128), f32),
         V((seg, 4 * kcols), bf16),
-        V((tok, 4 * qcols), bf16),
+        V((2 * own, 4 * qcols), bf16),
         V(query_up_weight.shape, bf16),
         V(key_up_weight.shape, bf16),
         V(value_up_weight.shape, bf16),
@@ -989,7 +994,6 @@
         V((seg, 128), f32),
         V((2 * own, modw), f32),
         V((2 * own, modw), f32),
-        V((own, width), bf16),
         DMA((18,)),
         DMA((48,)),
         DMA((48,)),
@@ -997,13 +1001,12 @@
         DMA((2, 2, spn)),
         DMA((3, 2, spn)),
         DMA((3, 2, spn)),
-        DMA((4,)),
     ]
     return pl.pallas_call(
         block_kernel,
-        out_shape=jax.ShapeDtypeStruct(latents.shape, bf16),
+        out_shape=pltpu.VMEM(latents.shape, bf16),
         in_specs=[hbm] * 18,
-        out_specs=hbm,
+        out_specs=pl.BlockSpec(memory_space=pltpu.VMEM),
         scratch_shapes=scratch,
         compiler_params=pltpu.CompilerParams(
             collective_id=0, has_side_effects=True, vmem_limit_bytes=56 * 1024 * 1024
@@ -1034,6 +1037,7 @@
     latents, context, bias = arrays[0], arrays[2], arrays[14]
     fits = (
         lax.axis_size("tp") == 4
+        and lax.axis_size("sp") == 4
         and latents.shape[0] % 32 == 0
         and context.shape[0] % 128 == 0
         and latents.shape[0] > 2 * BAND

time: 75.5 us -> 68.9 us (0.913)
  Pallas kernels: 73.3 us -> 67.9 us
  local copies, waits for them, and re-layouts: 2.06 us -> 0.88 us
    pallas_call x1, Pallas kernels: 73.3 us -> 67.9 us  [fused_device(): pl.pallas_call(block_kernel, out_shape=pltpu.VMEM(latents.shape, bf16), i...]
    unnamed x1, local copies, waits for them, and re-layouts: 2.06 us -> 0.88 us
where the time goes in v2:
time: 68.9 us; the launch traced here: 68.8 us
  Pallas kernels  67.9 us (99%)
  local copies, waits for them, and re-layouts  0.88 us (1%)
    pallas_call x1, Pallas kernels, fused_device(): pl.pallas_call(block_kernel, out_shape=pltpu.VMEM(latents.shape, bf16), i...  67.9 us

profile of v2, /device:TPU:0, one launch (start us, length us, event | category | flops | bytes accessed | tf_op | source)
XLA Modules:
  0.0 68.8 jit_solution(9551426068967716467)
XLA Ops:
  0.0 67.9 %shard_map.172 = bf16[96,4096]{1,0:T(8,128)(2,1)S(1)} custom-call(f32[2,1024]{1,0:T(2,128)} %cond_hbm.1, f32[8]{0:T(128)} %bias_hbm.1, f32[1,1024]{1,0:T(1,128)} %bitcast.4, f32[1,512]{1,0:T(1,128)} %bitcast.5, bf16[32,4096]{1,0:T(8,128)(2,1)} %bitcast.3, bf16[96,4096]{1,0:T(8,128)(2,1)} %lat_hbm.1, bf16[128,4096]{1,0:T(8,128)(2,1)} %ctx_hbm.1, ...), custom_call_target="tpu_custom_call" | custom-call | tf_op jit(solution)/shard_map/pallas_call | solution.py:1005
  67.9 0.9 %copy.20 = bf16[96,4096]{1,0:T(8,128)(2,1)} copy(bf16[96,4096]{1,0:T(8,128)(2,1)S(1)} %shard_map.172) | data formatting | bytes 1572864

commit v3 on v2

--- a/solution.py
+++ b/solution.py
@@ -524,13 +524,14 @@
         return krx.at[o, pl.ds(first // 4, count // 4)]
 
     class Hop:
-        def __init__(self, origin, target, way, part):
+        def __init__(self, origin, target, way, part, lane_of=None):
+            lane_of = origin if lane_of is None else lane_of
             views = (kv_piece(origin, p, part), kr_piece(origin, part))
             self.copies = [
                 copy_to(
                     view,
                     view,
-                    zsend.at[way, part, kind, origin],
+                    zsend.at[way, part, kind, lane_of],
                     zrecv.at[part, kind, origin],
                     {"sp": target},
                 )
@@ -582,15 +583,30 @@
         def _():
             fn(right, 1, z - 1, has_left)
 
+    def passed_on(step):
+        return step + 2 < spn - 1
+
+    def at_far_end(fn):
+        at_distance(spn - 2, lambda target, way, onward, more: fn(target, 1 - way))
+
     def forward(step, part):
         def one(o, way, onward, more):
             Hop(o, z, way, part).wait_recv()
-
-            @pl.when(more)
-            def _():
-                Hop(o, onward, way, part).start()
+            if passed_on(step):
+
+                @pl.when(more)
+                def _():
+                    Hop(o, onward, way, part).start()
 
         at_distance(step, one)
+
+    def at_distances(fn):
+        for step in range(spn - 1):
+            at_distance(step, lambda target, way, onward, more: fn(target, 1 - way))
+
+    def arrive(o):
+        Hop(o, z, 0, 1).wait_recv()
+        spread(o, 1)
 
     def down_kv(part):
         first, count = spans[part]
@@ -611,13 +627,19 @@
             krx[z, STEP * t : STEP * t + STEP, :] = packed.astype(bf16)
         spread(z, part)
 
-        @pl.when(has_right)
-        def _():
-            Hop(z, z + 1, 0, part).start()
-
-        @pl.when(has_left)
-        def _():
-            Hop(z, z - 1, 1, part).start()
+        if part == 0:
+
+            @pl.when(has_right)
+            def _():
+                Hop(z, z + 1, 0, part).start()
+
+            @pl.when(has_left)
+            def _():
+                Hop(z, z - 1, 1, part).start()
+
+            at_far_end(lambda target, way: Hop(z, target, way, part, target).start())
+        else:
+            at_distances(lambda target, way: Hop(z, target, way, part, target).start())
 
     def down_q(part):
         first, count = spans[part]
@@ -656,7 +678,7 @@
             gain = gain_ref[0:1, j * cols : (j + 1) * cols]
             store(slice(j * cols, (j + 1) * cols), (v * factor * gain).astype(bf16))
 
-    def expand_half(block, hf):
+    def expand_half(block, hf, slot=0):
         hrow = seg // 2
         for base in range(hf * hrow, (hf + 1) * hrow, 64):
             def put(cols, value, base=base):
@@ -665,6 +687,7 @@
             rms([kvx[block, r, base : base + 64, :] for r in range(4)], kvgain_ref, put)
         lane_h = lanes_of((hrow, 128))
         ones = (lane_h == VALUE_DIM).astype(f32)
+        ones_odd = (lane_h == 0).astype(f32)
         lane_s = lanes_of((STEP, 128))
         on_rope = (lane_s >= PLAIN_QK_DIM) & (lane_s < PLAIN_QK_DIM + ROTARY_DIM)
         rows = slice(hf * hrow, (hf + 1) * hrow)
@@ -676,19 +699,17 @@
                 moved = pltpu.roll(packed, (192 - 32 * j) % 128, 1)
                 pieces.append(jnp.where(on_rope, moved, 0.0))
         rope_key = jnp.concatenate(pieces, axis=0)
+        rope_odd = pltpu.roll(rope_key, 64, 1)
         keys = jnp.dot(latent_rows, wku[...], preferred_element_type=f32)
         vals = jnp.dot(latent_rows, wvu[...], preferred_element_type=f32)
         for hp in range(heads // 2):
             cols = slice(128 * hp, 128 * hp + 128)
             k2, v2 = keys[:, cols], vals[:, cols]
-            kb[2 * hp, rows, :] = jnp.where(lane_h < 64, k2, rope_key).astype(bf16)
-            kb[2 * hp + 1, rows, :] = jnp.where(
-                lane_h < 64, pltpu.roll(k2, 64, 1), rope_key
-            ).astype(bf16)
-            vb[2 * hp, rows, :] = jnp.where(lane_h < 64, v2, ones).astype(bf16)
-            vb[2 * hp + 1, rows, :] = jnp.where(
-                lane_h < 64, pltpu.roll(v2, 64, 1), ones
-            ).astype(bf16)
+            even, odd = slot * heads + 2 * hp, slot * heads + 2 * hp + 1
+            kb[even, rows, :] = jnp.where(lane_h < 64, k2, rope_key).astype(bf16)
+            kb[odd, rows, :] = jnp.where(lane_h < 64, rope_odd, k2).astype(bf16)
+            vb[even, rows, :] = jnp.where(lane_h < 64, v2, ones).astype(bf16)
+            vb[odd, rows, :] = jnp.where(lane_h < 64, ones_odd, v2).astype(bf16)
 
     def block_at(step):
         below = jnp.minimum(z, spn - 1 - z)
@@ -717,7 +738,14 @@
                     head = jnp.where(
                         lane < 128 - shift, head, pltpu.roll(rest, 128 - shift, 1)
                     )
-            qh[h, rows, :] = turned(head, cosv[rows, :], sinv[rows, :]).astype(bf16)
+            head = turned(head, cosv[rows, :], sinv[rows, :])
+            if h % 2:
+                head = pltpu.roll(head, 64, 1)
+            head = head.astype(bf16)
+            for which in range(2):
+                qh[h, which ^ side, b * own : (b + 1) * own, :] = head[
+                    which * own : (which + 1) * own
+                ]
 
     for copy in l_small:
         copy.wait()
@@ -736,120 +764,134 @@
         w()
     up_q(0)
     forward(1, 0)
+    cq_waits = [cq_b[1], cq_b[0]()]
     gathered(z, 0)
     expand_half(z, 0)
-    cq_waits = [cq_b[1], cq_b[0]()]
     relay(z, 1)
-    forward(0, 1)
-    spread(blocks[1], 1)
+    arrive(blocks[1])
     spread(blocks[2], 0)
     for w in cq_waits:
         w()
     up_q(1)
     gathered(z, 1)
     expand_half(z, 1)
-
-    def score(h):
-        return lax.dot_general(
-            qh[h], kb[h], (((1,), (1,)), ((), ())), preferred_element_type=f32
-        )
-
-    def attend(h, scores):
-        tiles = [scores[:, c : c + 128] * factor for c in range(0, seg, 128)]
+    at_end = jnp.logical_not(jnp.logical_and(has_left, has_right))
+
+    @pl.when(jnp.logical_not(at_end))
+    def _():
+        arrive(blocks[2])
+
+    def rows_of(ref, h, group):
+        return ref[h].reshape(tok, 128) if group is None else ref[h, group]
+
+    def score(h, group, slots):
+        return [
+            lax.dot_general(
+                rows_of(qh, h, group),
+                kb[slot * heads + h],
+                (((1,), (1,)), ((), ())),
+                preferred_element_type=f32,
+            )
+            for slot in slots
+        ]
+
+    def attend(h, scores, group, slots):
         bias = bias_ref[h] * LOG2E
-        tiles = [t + bias if n * 128 < ctxn else t for n, t in enumerate(tiles)]
+        tiles = []
+        for part_scores in scores:
+            for c in range(0, seg, 128):
+                tile = part_scores[:, c : c + 128] * factor
+                tiles.append(tile + bias if c < ctxn else tile)
         best = functools.reduce(jnp.maximum, tiles)
-        old = mx[h]
+        old = rows_of(mx, h, group)
         new = jnp.maximum(old, jnp.max(best, axis=-1, keepdims=True))
-        mx[h] = new
-        weights = jnp.concatenate([jnp.exp2(t - new).astype(bf16) for t in tiles], axis=1)
-        acc[h] = acc[h] * jnp.exp2(old - new) + jnp.dot(
-            weights, vb[h], preferred_element_type=f32
-        )
-
-    def attend_all(after):
-        scores = score(0)
+        total = rows_of(acc, h, group) * jnp.exp2(old - new)
+        each = seg // 128
+        for n, slot in enumerate(slots):
+            weights = jnp.concatenate(
+                [jnp.exp2(t - new).astype(bf16) for t in tiles[n * each : (n + 1) * each]],
+                axis=1,
+            )
+            total = total + jnp.dot(weights, vb[slot * heads + h], preferred_element_type=f32)
+        if group is None:
+            mx[h] = new.reshape(2, pair, 128)
+            acc[h] = total.reshape(2, pair, 128)
+        else:
+            mx[h, group] = new
+            acc[h, group] = total
+
+    def attend_all(after, group=None, slots=(0,)):
+        scores = score(0, group, slots)
         for h in range(heads):
-            following = score(h + 1) if h + 1 < heads else None
-            attend(h, scores)
+            following = score(h + 1, group, slots) if h + 1 < heads else None
+            attend(h, scores, group, slots)
             after(h)
             scores = following
 
     @pl.loop(1, spn)
     def _(step):
         block = block_at(step)
+        final_step = step == spn - 1
 
         def meanwhile(h):
             if h != RELAY_AFTER:
                 return
 
+            for part in range(2):
+                relay(block, part)
+
             @pl.when(step == 1)
             def _():
+                @pl.when(at_end)
+                def _():
+                    arrive(blocks[2])
+
                 forward(2, 0)
-                forward(1, 1)
-                spread(blocks[2], 1)
                 spread(blocks[3], 0)
-
-            for part in range(2):
-                relay(block, part)
-
-            @pl.when(step == 2)
-            def _():
-                forward(2, 1)
-                spread(blocks[3], 1)
-
-        attend_all(meanwhile)
+                arrive(blocks[3])
+
+        @pl.when(jnp.logical_not(final_step))
+        def _():
+            attend_all(meanwhile)
+
+        @pl.when(final_step)
+        def _():
+            attend_all(meanwhile, 0)
+
         for part in range(2):
             gathered(block, part)
+        slot = jnp.where(final_step, 1, 0)
         for hf in range(2):
-            expand_half(block, hf)
+            expand_half(block, hf, slot)
 
     att_relay, att_near = [], []
-    lane64 = lanes_of((tok, 128)) < VALUE_DIM
-    quarter = own
-
-    def finish(h):
+    hps = heads // 2
+    lane64 = lanes_of((pair, 128)) < VALUE_DIM
+
+    def finish(h, group):
         if h % 2 == 0:
             return
         hp = h // 2
-        low, high = acc[h - 1], acc[h]
-        totals = jnp.where(
-            lane64, low[:, VALUE_DIM : VALUE_DIM + 1], high[:, VALUE_DIM : VALUE_DIM + 1]
-        )
-        value = (jnp.where(lane64, low, pltpu.roll(high, 64, 1)) / totals).astype(bf16)
-        for b in range(2):
-            for s in range(2):
-                row = (2 * b + s) * quarter
-                att[p, hp, b, s] = value[row : row + quarter]
+        low, high = acc[h - 1, group], acc[h, group]
+        totals = jnp.where(lane64, low[:, VALUE_DIM : VALUE_DIM + 1], high[:, 0:1])
+        att[p, hp, side ^ group] = (jnp.where(lane64, low, high) / totals).astype(bf16)
         att_relay.append(
             far(
-                lambda slot: att.at[slot, hp, :, side],
-                lambda slot: att.at[slot, hp, :, 1 - side],
+                lambda slot: att.at[slot, hp, side ^ group],
+                lambda slot: att.at[slot, hp, 1 - (side ^ group)],
             )
         )
-        att_near.append(near(lambda slot: att.at[slot, hp]))
-
-    attend_all(finish)
-
-    hps = heads // 2
-    for first in range(0, hps, 2):
-        att_relay.append(
-            far(
-                lambda slot, first=first: att.at[slot, pl.ds(first, 2), :, 1 - side],
-                lambda slot, first=first: att.at[slot, pl.ds(first, 2), :, side],
-            )
-        )
+        att_near.append(near(lambda slot: att.at[slot, hp, side ^ group]))
+
+    attend_all(lambda h: finish(h, 0), 0, (1,))
+    attend_all(lambda h: finish(h, 1), 1, (0, 1))
+
     l_wo.wait()
     half_k = heads * VALUE_DIM * 2
 
     def project(rows_side, chip):
         joined = jnp.concatenate(
-            [
-                jnp.concatenate([att[2 * chip + r, hp, b, rows_side] for b in range(2)], axis=0)
-                for r in range(2)
-                for hp in range(hps)
-            ],
-            axis=1,
+            [att[2 * chip + r, hp, rows_side] for r in range(2) for hp in range(hps)], axis=1
         )
         k_rows = pl.ds(pl.multiple_of(chip * half_k, 128), half_k)
         return jnp.dot(joined, wo[k_rows, :], preferred_element_type=f32)
@@ -904,24 +946,28 @@
         for kind in range(3):
             swap(z, part, kind).wait_send()
 
-        @pl.when(has_right)
-        def _():
-            Hop(z, z + 1, 0, part).wait_send()
-
-        @pl.when(has_left)
-        def _():
-            Hop(z, z - 1, 1, part).wait_send()
-
-        def drain(o, way, onward, more):
+        def drain(o, way, onward, more, step=0):
             for kind in range(3):
                 swap(o, part, kind).wait_send()
-
-            @pl.when(more)
-            def _():
-                Hop(o, onward, way, part).wait_send()
+            if part == 0 and passed_on(step):
+
+                @pl.when(more)
+                def _():
+                    Hop(o, onward, way, part).wait_send()
 
         for step in range(spn - 1):
-            at_distance(step, drain)
+            at_distance(step, functools.partial(drain, step=step))
+
+    @pl.when(has_right)
+    def _():
+        Hop(z, z + 1, 0, 0).wait_send()
+
+    @pl.when(has_left)
+    def _():
+        Hop(z, z - 1, 1, 0).wait_send()
+
+    at_far_end(lambda target, way: Hop(z, target, way, 0, target).wait_send())
+    at_distances(lambda target, way: Hop(z, target, way, 1, target).wait_send())
 
 
 def fused_device(
@@ -982,12 +1028,12 @@
         V(w_out.shape, bf16),
         V((tok, 128), f32),
         V((tok, 128), f32),
-        V((heads, tok, 128), bf16),
-        V((heads, seg, 128), bf16),
-        V((heads, seg, 128), bf16),
-        V((heads, tok, 128), f32),
-        V((heads, tok, 128), f32),
-        V((4, heads // 2, 2, 2, own, 128), bf16),
+        V((heads, 2, 2 * own, 128), bf16),
+        V((2 * heads, seg, 128), bf16),
+        V((2 * heads, seg, 128), bf16),
+        V((heads, 2, 2 * own, 128), f32),
+        V((heads, 2, 2 * own, 128), f32),
+        V((4, heads // 2, 2, 2 * own, 128), bf16),
         V((4, own, modw), bf16),
         V((4, own, modw), bf16),
         V((seg, 128), f32),
@@ -995,8 +1041,8 @@
         V((2 * own, modw), f32),
         V((2 * own, modw), f32),
         DMA((18,)),
-        DMA((48,)),
-        DMA((48,)),
+        DMA((64,)),
+        DMA((64,)),
         DMA((2, 2, 2, spn)),
         DMA((2, 2, spn)),
         DMA((3, 2, spn)),

time: 68.9 us -> 68.2 us (0.990)
  Pallas kernels: 67.9 us -> 67.2 us
    pallas_call x1, Pallas kernels: 67.9 us -> 67.2 us  [fused_device(): pl.pallas_call(block_kernel, out_shape=pltpu.VMEM(latents.shape, bf16), i...]
where the time goes in v3:
time: 68.2 us; the launch traced here: 68.1 us
  Pallas kernels  67.2 us (99%)
  local copies, waits for them, and re-layouts  0.88 us (1%)
    pallas_call x1, Pallas kernels, fused_device(): pl.pallas_call(block_kernel, out_shape=pltpu.VMEM(latents.shape, bf16), i...  67.2 us

profile of v3, /device:TPU:0, one launch (start us, length us, event | category | flops | bytes accessed | tf_op | source)
XLA Modules:
  0.0 68.1 jit_solution(2970317789554927030)
XLA Ops:
  0.0 67.2 %shard_map.172 = bf16[96,4096]{1,0:T(8,128)(2,1)S(1)} custom-call(f32[2,1024]{1,0:T(2,128)} %cond_hbm.1, f32[8]{0:T(128)} %bias_hbm.1, f32[1,1024]{1,0:T(1,128)} %bitcast.4, f32[1,512]{1,0:T(1,128)} %bitcast.5, bf16[32,4096]{1,0:T(8,128)(2,1)} %bitcast.3, bf16[96,4096]{1,0:T(8,128)(2,1)} %lat_hbm.1, bf16[128,4096]{1,0:T(8,128)(2,1)} %ctx_hbm.1, ...), custom_call_target="tpu_custom_call" | custom-call | tf_op jit(solution)/shard_map/pallas_call | solution.py:1051
  67.2 0.9 %copy.20 = bf16[96,4096]{1,0:T(8,128)(2,1)} copy(bf16[96,4096]{1,0:T(8,128)(2,1)S(1)} %shard_map.172) | data formatting | bytes 1572864
